TPU v7x, 32 devices: a whole 2x2x4 slice. The times are simulated.
32 devices in a mesh: sp: 16 (over z, y, x), tp: 2 (over core).
Axes of the slice: x: 2, y: 2, z: 4, core: 2. Of those that a mesh axis runs over, the one named last changes fastest.
Arguments:
- tokens: bfloat16 [4096, 4096], P('sp', 'tp'), may hold values from -480 to 480
- gain: float32 [4096], P('tp'), may hold values from 0.1 to 1.9
- q_att: bfloat16 [4096, 2048], P('sp', 'tp'), may hold values from -2.90625 to 2.90625
- k_att: bfloat16 [4096, 1024], P('sp', 'tp'), may hold values from -0.09375 to 0.09375
- v_att: bfloat16 [4096, 1024], P('sp', 'tp'), may hold values from -0.75 to 0.75
- q_ret: bfloat16 [4096, 1024], P('sp', 'tp'), may hold values from -0.09375 to 0.09375
- k_ret: bfloat16 [4096, 1024], P('sp', 'tp'), may hold values from -0.09375 to 0.09375
- v_ret: bfloat16 [4096, 1024], P('sp', 'tp'), may hold values from -0.09375 to 0.09375
- out_att: bfloat16 [2048, 4096], P('tp', 'sp'), may hold values from -0.109375 to 0.109375
- out_ret: bfloat16 [1024, 4096], P('tp', 'sp'), may hold values from -0.109375 to 0.109375
- sink: float32 [16], P('tp'), may hold values from 3 to 7
- decay_log: float32 [8, 4096], P('tp', 'sp'), may hold values from -2.125 to 0
Outputs:
- mixed: bfloat16 [4096, 4096], P(('sp', 'tp'))
- log_weight: float32 [16, 4096], P('tp', 'sp')
All inputs are finite; a program needn't handle non-finite values.
Results may differ from a plain program's by a relative error of at most 0.017.
Values may be sent and summed in bfloat16 or wider, within the bound.
A program may use at most 128 MiB of HBM per device.

v0:
```python
import functools
import math

import jax
import jax.numpy as jnp
from jax import lax
from jax.experimental import pallas as pl
from jax.experimental.pallas import tpu as pltpu
from jax.sharding import Mesh
from jax.sharding import PartitionSpec as P

HEAD_DIM = 128
SPAN_RADIUS = 128
BLOCK = 256
HIGHEST = lax.Precision.HIGHEST
MESH = pl.DeviceIdType.MESH


def gather(x, axis, dim):
    if lax.axis_size(axis) == 1:
        return x
    return lax.all_gather(x, axis, axis=dim, tiled=True)


def exchange(x, axis, split, concat):
    if lax.axis_size(axis) == 1:
        return x
    return lax.all_to_all(x, axis, split, concat, tiled=True)


def halo(shard, axis, width):
    peers, length = lax.axis_size(axis), shard.shape[1]
    up = [(i, i + 1) for i in range(peers - 1)]
    down = [(j, i) for i, j in up]
    before = lax.ppermute(shard[:, length - width :], axis, up)
    after = lax.ppermute(shard[:, :width], axis, down)
    return jnp.concatenate([before, shard, after], axis=1)


def rotate(values, cosine, sine):
    half = values.shape[-1] // 2
    first, second = values[..., :half], values[..., half:]
    return jnp.concatenate(
        [first * cosine - second * sine, second * cosine + first * sine], axis=-1
    ).astype(jnp.bfloat16)


def front_kernel(
    peers, parts, cores,
    packed, scaled, sums, outp, decay,
    proj, out_all, sums_all, decay_all,
    wide, seen,
    w_recv, up_send, down_send, w_send,
    x_recv, x_send, swap_send,
    s_recv, s_send, o_recv, o_send, d_recv, d_send, local,
):
    t, h, c = lax.axis_index("t"), lax.axis_index("h"), lax.axis_index("tp")
    blocks, own, _ = scaled.shape

    def other(d):
        return lax.rem(h + d, parts)

    def source(d):
        return lax.rem(h - d + parts, parts)

    barrier = pltpu.get_barrier_semaphore()
    for d in range(parts):
        for e in range(cores):
            if d or e:
                pl.semaphore_signal(
                    barrier,
                    inc=1,
                    device_id={"h": other(d), "tp": lax.rem(c + e, cores)},
                    device_id_type=MESH,
                )

    for d in range(1, peers):
        pl.semaphore_signal(
            barrier, inc=1, device_id={"t": lax.rem(t + d, peers)}, device_id_type=MESH
        )
    pl.semaphore_wait(barrier, parts * cores + peers - 2)

    def remote(src, dst, send, recv, where):
        return pltpu.make_async_remote_copy(
            src_ref=src, dst_ref=dst, send_sem=send, recv_sem=recv,
            device_id=where, device_id_type=MESH,
        )

    def upward(b, p, src=None):
        return remote(
            wide.at[b, p] if src is None else src,
            wide.at[b, p], up_send.at[b, p], w_recv.at[b, p], {"t": t + 1},
        )

    def downward(b, p, src=None):
        return remote(
            wide.at[b, p] if src is None else src,
            wide.at[b, p], down_send.at[b, p], w_recv.at[b, p], {"t": t - 1},
        )

    def weight_to(d):
        return remote(
            packed.at[other(d)], wide.at[t, h], w_send.at[d], w_recv.at[t, h], {"h": other(d)}
        )

    def place(p, e):
        return seen.at[pl.ds(e * blocks, blocks), pl.ds(p * own, own)]

    def token_to(d):
        return remote(scaled, place(h, c), x_send.at[d], x_recv.at[h, c], {"h": other(d)})

    def swap(p, src):
        return remote(
            src, place(p, c), swap_send.at[p], x_recv.at[p, c], {"tp": lax.rem(c + 1, cores)}
        )

    def sum_to(d, e):
        return remote(
            sums, sums_all.at[h, c], s_send.at[d, e], s_recv.at[h, c],
            {"h": other(d), "tp": lax.rem(c + e, cores)},
        )

    def out_to(d):
        return remote(
            outp.at[other(d)], out_all.at[h], o_send.at[d], o_recv.at[h], {"h": other(d)}
        )

    def decay_to(d):
        return remote(
            decay.at[other(d)], decay_all.at[h], d_send.at[d], d_recv.at[h], {"h": other(d)}
        )

    for d in range(1, parts):
        weight_to(d).start()

    @pl.when(t < peers - 1)
    def _():
        upward(t, h, packed.at[h]).start()

    @pl.when(t > 0)
    def _():
        downward(t, h, packed.at[h]).start()

    for d in range(1, parts):
        token_to(d).start()
    swap(h, scaled).start()
    for d in range(1, parts):
        decay_to(d).start()
        out_to(d).start()
    for d in range(parts):
        for e in range(cores):
            if d or e:
                sum_to(d, e).start()
    mine = (
        pltpu.make_async_copy(packed.at[h], wide.at[t, h], local.at[0]),
        pltpu.make_async_copy(scaled, place(h, c), local.at[1]),
        pltpu.make_async_copy(sums, sums_all.at[h, c], local.at[2]),
        pltpu.make_async_copy(outp.at[h], out_all.at[h], local.at[3]),
        pltpu.make_async_copy(decay.at[h], decay_all.at[h], local.at[4]),
    )
    for copy in mine:
        copy.start()
    proj[...] = jnp.zeros_like(proj)

    @pl.loop(1, parts)
    def _(d):
        p = source(d)
        upward(t, p).wait_recv()

        @pl.when(t < peers - 1)
        def _():
            upward(t, p).start()

        @pl.when(t > 0)
        def _():
            downward(t, p).start()

    def relay(s, d):
        p = source(d)

        @pl.when(t - s >= 0)
        def _():
            upward(t - s, p).wait_recv()

            @pl.when(t < peers - 1)
            def _():
                upward(t - s, p).start()

        @pl.when(t + s < peers)
        def _():
            downward(t + s, p).wait_recv()

            @pl.when(t > 0)
            def _():
                downward(t + s, p).start()

    @pl.loop(0, parts)
    def _(d):
        relay(1, d)

        @pl.when(d < parts - 1)
        def _():
            p = source(d + 1)
            swap(p, place(p, c)).wait_recv()
            swap(p, place(p, c)).start()

    for copy in mine:
        copy.wait()

    @pl.loop(0, parts)
    def _(p):
        e = lax.rem(c + 1, cores)
        pltpu.make_async_remote_copy(
            src_ref=place(p, e), dst_ref=place(p, e),
            send_sem=swap_send.at[p], recv_sem=x_recv.at[p, e],
            device_id={"tp": e}, device_id_type=MESH,
        ).wait_recv()

    def add(b, p):
        @pl.loop(0, parts)
        def _(r):
            at = pl.ds(pl.multiple_of(r * own, own), own)
            proj[at, :] += jnp.dot(
                seen[b * parts + p, at, :], wide[b, p], preferred_element_type=jnp.float32
            )

    @pl.loop(0, peers)
    def _(s):
        @pl.loop(0, parts)
        def _(d):
            p = source(d)

            @pl.when(s >= 2)
            def _():
                relay(s, d)

            @pl.when(t - s >= 0)
            def _():
                add(t - s, p)

            @pl.when((s > 0) & (t + s < peers))
            def _():
                add(t + s, p)

    @pl.loop(0, peers)
    def _(b):
        @pl.loop(0, parts)
        def _(p):
            @pl.when((b <= t) & (t < peers - 1))
            def _():
                upward(b, p).wait_send()

            @pl.when((b >= t) & (t > 0))
            def _():
                downward(b, p).wait_send()

    for p in range(parts):
        swap(p, place(p, c)).wait_send()
    for d in range(parts):
        if d:
            p = source(d)
            weight_to(d).wait_send()
            token_to(d).wait_send()
            out_to(d).wait_send()
            decay_to(d).wait_send()
            remote(
                outp.at[h], out_all.at[p], o_send.at[d], o_recv.at[p], {"h": p}
            ).wait_recv()
            remote(
                decay.at[h], decay_all.at[p], d_send.at[d], d_recv.at[p], {"h": p}
            ).wait_recv()
        for e in range(cores):
            if d or e:
                p, q = source(d), lax.rem(c + e, cores)
                sum_to(d, e).wait_send()
                remote(
                    sums, sums_all.at[p, q], s_send.at[d, e], s_recv.at[p, q],
                    {"h": p, "tp": q},
                ).wait_recv()


def front(packed, scaled, sums, outp, decay):
    peers, parts, cores = (lax.axis_size(a) for a in ("t", "h", "tp"))
    own, columns = packed.shape[1:]
    dma = pltpu.SemaphoreType.DMA
    vmem = pl.BlockSpec(memory_space=pltpu.VMEM)
    rows = parts * own
    return pl.pallas_call(
        functools.partial(front_kernel, peers, parts, cores),
        out_shape=(
            jax.ShapeDtypeStruct((rows, columns), jnp.float32),
            jax.ShapeDtypeStruct(outp.shape, outp.dtype),
            jax.ShapeDtypeStruct((parts, cores) + sums.shape, sums.dtype),
            jax.ShapeDtypeStruct(decay.shape, decay.dtype),
        ),
        in_specs=[vmem] * 5,
        out_specs=[vmem] * 4,
        scratch_shapes=[
            pltpu.VMEM((peers, parts, own, columns), jnp.bfloat16),
            pltpu.VMEM((cores * scaled.shape[0], rows, own), jnp.bfloat16),
            dma((peers, parts)), dma((peers, parts)), dma((peers, parts)), dma((parts,)),
            dma((parts, cores)), dma((parts,)), dma((parts,)),
            dma((parts, cores)), dma((parts, cores)),
            dma((parts,)), dma((parts,)), dma((parts,)), dma((parts,)), dma((5,)),
        ],
        compiler_params=pltpu.CompilerParams(
            collective_id=0, has_side_effects=True, vmem_limit_bytes=56 * 2**20
        ),
        cost_estimate=pl.CostEstimate(
            flops=10**11, bytes_accessed=2 * 10**7, transcendentals=0
        ),
    )(packed, scaled, sums, outp, decay)


def back_kernel(
    parts, cores, mixers, wide, logs, mixed, logs_all,
    give, take, mine, total, seen,
    give_send, take_recv, total_send, seen_recv, l_send, l_recv, local,
):
    h, c = lax.axis_index("h"), lax.axis_index("tp")
    partner = lax.rem(c + 1, cores)
    half = mixed.shape[0]
    count, _, tile = wide.shape

    def other(d):
        return lax.rem(h + d, parts)

    barrier = pltpu.get_barrier_semaphore()
    for d in range(1, parts):
        pl.semaphore_signal(barrier, inc=1, device_id={"h": other(d)}, device_id_type=MESH)
    pl.semaphore_signal(barrier, inc=1, device_id={"tp": partner}, device_id_type=MESH)
    pl.semaphore_wait(barrier, parts)

    def remote(src, dst, send, recv, where):
        return pltpu.make_async_remote_copy(
            src_ref=src, dst_ref=dst, send_sem=send, recv_sem=recv,
            device_id=where, device_id_type=MESH,
        )

    def swap(d):
        return remote(give.at[d], take.at[d], give_send.at[d], take_recv.at[d], {"tp": partner})

    def scatter(d):
        return remote(
            total.at[d], seen.at[d], total_send.at[d], seen_recv.at[d], {"h": other(d)}
        )

    def log_to(d):
        return remote(
            logs.at[other(d)], logs_all.at[h], l_send.at[d], l_recv.at[h], {"h": other(d)}
        )

    for d in range(1, parts):
        log_to(d).start()
    own_logs = pltpu.make_async_copy(logs.at[h], logs_all.at[h], local.at[0])
    own_logs.start()

    def project(d):
        at = pl.ds(pl.multiple_of(other(d) * 2 * half, 2 * half), 2 * half)

        @pl.loop(0, count)
        def _(j):
            columns = pl.ds(pl.multiple_of(j * tile, tile), tile)
            part = jnp.dot(mixers[at, :], wide[j], preferred_element_type=jnp.float32)
            low, high = part[:half], part[half:]
            give[d, :, columns] = jnp.where(c == 0, high, low).astype(give.dtype)
            mine[d, :, columns] = jnp.where(c == 0, low, high)

    def settle(d):
        swap(d).wait_recv()
        total[d] = (mine[d] + take[d].astype(jnp.float32)).astype(total.dtype)
        scatter(d).start()

    @pl.loop(1, parts + 1)
    def _(i):
        d = lax.rem(i, parts)
        project(d)
        swap(d).start()

        @pl.when(i > 1)
        def _():
            settle(i - 1)

    swap(0).wait_recv()
    mine[0] = mine[0] + take[0].astype(jnp.float32)

    @pl.loop(1, parts)
    def _(d):
        scatter(d).wait_recv()
        mine[0] += seen[d].astype(jnp.float32)

    mixed[...] = mine[0].astype(mixed.dtype)

    own_logs.wait()
    for d in range(parts):
        swap(d).wait_send()
        if d:
            scatter(d).wait_send()
            log_to(d).wait_send()
            p = lax.rem(h - d + parts, parts)
            remote(
                logs.at[h], logs_all.at[p], l_send.at[d], l_recv.at[p], {"h": p}
            ).wait_recv()


def back(mixers, wide, logs):
    parts, cores = lax.axis_size("h"), lax.axis_size("tp")
    half = mixers.shape[0] // parts // cores
    columns = wide.shape[0] * wide.shape[2]
    dma = pltpu.SemaphoreType.DMA
    vmem = pl.BlockSpec(memory_space=pltpu.VMEM)
    block = (parts, half, columns)
    return pl.pallas_call(
        functools.partial(back_kernel, parts, cores),
        out_shape=(
            jax.ShapeDtypeStruct((half, columns), jnp.bfloat16),
            jax.ShapeDtypeStruct(logs.shape, logs.dtype),
        ),
        in_specs=[vmem] * 3,
        out_specs=[vmem] * 2,
        scratch_shapes=[
            pltpu.VMEM(block, jnp.bfloat16), pltpu.VMEM(block, jnp.bfloat16),
            pltpu.VMEM(block, jnp.float32),
            pltpu.VMEM(block, jnp.bfloat16), pltpu.VMEM(block, jnp.bfloat16),
        ]
        + [dma((parts,))] * 6
        + [dma((1,))],
        compiler_params=pltpu.CompilerParams(
            collective_id=1, has_side_effects=True, vmem_limit_bytes=56 * 2**20
        ),
        cost_estimate=pl.CostEstimate(
            flops=5 * 10**10, bytes_accessed=2 * 10**7, transcendentals=0
        ),
    )(mixers, wide, logs)


def attend(query, key, value, sink, offset, total_rows):
    rows, kv, group, _ = query.shape
    ext = halo(jnp.stack([key, value]), "t", SPAN_RADIUS)
    size = min(rows, BLOCK)
    count = rows // size
    span = size + 2 * SPAN_RADIUS
    pieces = jnp.stack([ext[:, b * size : b * size + span] for b in range(count)])
    blocks = query.reshape(count, size, kv, group, HEAD_DIM)
    scores = jnp.einsum(
        "bqhgd,bkhd->bhgqk", blocks, pieces[:, 0], preferred_element_type=jnp.float32
    ) * HEAD_DIM ** (-0.5)
    base = offset + jnp.arange(count, dtype=jnp.int32) * size
    query_pos = base[:, None] + jnp.arange(size, dtype=jnp.int32)
    key_pos = base[:, None] - SPAN_RADIUS + jnp.arange(span, dtype=jnp.int32)
    spacing = key_pos[:, None, :] - query_pos[:, :, None]
    inside = (key_pos >= 0) & (key_pos < total_rows)
    valid = (jnp.abs(spacing) <= SPAN_RADIUS) & inside[:, None, :]
    masked = jnp.where(valid[:, None, None], scores, -jnp.inf)
    limit = sink[None, :, :, None]
    top = jnp.maximum(jnp.max(masked, axis=-1), limit)
    expo = jnp.exp(masked - top[..., None])
    total = jnp.sum(expo, axis=-1) + jnp.exp(limit - top)
    logs = top + jnp.log(total)
    probs = (expo / total[..., None]).astype(jnp.bfloat16)
    result = jnp.einsum(
        "bhgqk,bkhd->bqhgd", probs, pieces[:, 1], preferred_element_type=jnp.float32
    ).astype(jnp.bfloat16)
    logs = jnp.transpose(logs, (1, 2, 0, 3)).reshape(kv * group, rows)
    return result.reshape(rows, kv * group * HEAD_DIM), logs


def retain(query, key, value, decay):
    rows, heads, _ = query.shape
    peers, index = lax.axis_size("t"), lax.axis_index("t")
    cumul = jnp.cumsum(decay, axis=1)
    last = cumul[:, -1]
    query_f, key_f, value_f = (v.astype(jnp.float32) for v in (query, key, value))
    trailing = jnp.exp(last[:, None] - cumul)
    leading = jnp.exp(cumul)
    forward = jnp.einsum("hk,khd,khe->hde", trailing, key_f, value_f, precision=HIGHEST)
    backward = jnp.einsum("hk,khd,khe->hde", leading, key_f, value_f, precision=HIGHEST)
    tail = jnp.broadcast_to(last[:, None, None], (heads, 8, HEAD_DIM))
    sent = jnp.concatenate([forward, backward, tail], axis=1)
    seen = lax.all_gather(sent, "t", axis=0)
    lasts = seen[:, :, 2 * HEAD_DIM, 0]
    at = jnp.arange(peers)
    low = jnp.minimum(at, index)[:, None]
    high = jnp.maximum(at, index)[:, None]
    between = (at[None, :] > low) & (at[None, :] < high)
    spans = jnp.exp(jnp.sum(jnp.where(between[:, :, None], lasts[None], 0.0), axis=1))
    before = jnp.sum(
        jnp.where(at < index, 1.0, 0.0)[:, None, None, None]
        * spans[:, :, None, None]
        * seen[:, :, :HEAD_DIM],
        axis=0,
    )
    after = jnp.sum(
        jnp.where(at > index, 1.0, 0.0)[:, None, None, None]
        * spans[:, :, None, None]
        * seen[:, :, HEAD_DIM : 2 * HEAD_DIM],
        axis=0,
    )
    scores = jnp.einsum("qhd,khd->hqk", query, key, preferred_element_type=jnp.float32)
    weights = jnp.exp(-jnp.abs(cumul[:, :, None] - cumul[:, None, :]))
    mix = jnp.einsum("hqk,khd->qhd", scores * weights, value_f, precision=HIGHEST)
    mix = mix + leading.T[:, :, None] * jnp.einsum(
        "qhd,hde->qhe", query_f, before, precision=HIGHEST
    )
    mix = mix + trailing.T[:, :, None] * jnp.einsum(
        "qhd,hde->qhe", query_f, after, precision=HIGHEST
    )
    middle = mix - jnp.mean(mix, axis=-1, keepdims=True)
    normed = middle * lax.rsqrt(jnp.mean(middle * middle, axis=-1, keepdims=True) + 1e-06)
    return normed.astype(jnp.bfloat16).reshape(rows, heads * HEAD_DIM)


def shards(
    tokens, gain, q_att, k_att, v_att, q_ret, k_ret, v_ret, out_att, out_ret, sink, decay_log
):
    parts = lax.axis_size("h")
    own = tokens.shape[0]
    rows = own * parts
    width = tokens.shape[1] * lax.axis_size("tp")
    kv = k_att.shape[1] // HEAD_DIM // parts
    group = q_att.shape[1] // k_att.shape[1]
    att = kv * group
    ret = q_ret.shape[1] // HEAD_DIM // parts
    offset = lax.axis_index("t") * rows
    total_rows = rows * lax.axis_size("t")

    packed = jnp.concatenate(
        [
            w.reshape(w.shape[0], parts, w.shape[1] // parts)
            for w in (q_att, k_att, v_att, q_ret, k_ret, v_ret)
        ],
        axis=2,
    )
    packed = jnp.moveaxis(packed, 1, 0)
    out_pack = jnp.concatenate(
        [w.reshape(parts, w.shape[0] // parts, w.shape[1]) for w in (out_att, out_ret)], axis=1
    )
    widened = tokens.astype(jnp.float32)
    sums = jnp.sum(widened * widened, axis=1)
    scaled = (widened * gain).astype(jnp.bfloat16)
    cores = lax.axis_size("tp")
    fused = parts > 1 and cores == 2 and own % 128 == 0 and packed.shape[1] == own
    if fused:
        tiles = jnp.moveaxis(scaled.reshape(own, -1, own), 1, 0)
        proj, out_own, sums, decay = front(
            packed, tiles, sums.reshape(-1, 128), out_pack, decay_log.reshape(parts, ret, own)
        )
        decay = jnp.moveaxis(decay, 0, 1).reshape(ret, rows)
    else:
        flat = packed.reshape(parts * packed.shape[1], packed.shape[2])
        weight = gather(exchange(flat, "h", 0, 0), "t", 0)
        whole = gather(gather(scaled, "h", 0), "tp", 1)
        proj = jnp.dot(whole, weight, preferred_element_type=jnp.float32)
        out_own = exchange(out_pack, "h", 0, 0)
        sums = lax.all_gather(sums, ("h", "tp"))
        decay = exchange(decay_log, "h", 0, 1)
    squares = jnp.sum(sums.reshape(parts, cores, own), axis=1).reshape(rows)
    inverse = lax.rsqrt(squares / width + 1e-06)[:, None]

    edges = [att, kv, kv, ret, ret, ret]
    starts = [sum(edges[:i]) * HEAD_DIM for i in range(6)]
    qa, ka, va, qr, kr, vr = (
        proj[:, s : s + n * HEAD_DIM].reshape(rows, n, HEAD_DIM) for s, n in zip(starts, edges)
    )
    scale = inverse[:, :, None]
    positions = (offset + jnp.arange(rows, dtype=jnp.int32)).astype(jnp.float32)
    freqs = 10000.0 ** (-jnp.arange(0, HEAD_DIM, 2).astype(jnp.float32) / HEAD_DIM)
    angles = positions[:, None] * freqs[None, :]
    cosine, sine = jnp.cos(angles)[:, None, :], jnp.sin(angles)[:, None, :]
    att_query = rotate(qa * scale, cosine, sine)
    att_key = rotate(ka * scale, cosine, sine)
    att_value = (va * scale).astype(jnp.bfloat16)
    ret_query = (qr * scale).astype(jnp.bfloat16)
    ret_key = (kr * (scale * HEAD_DIM ** (-0.5))).astype(jnp.bfloat16)
    ret_value = (vr * scale).astype(jnp.bfloat16)

    logits = lax.dynamic_slice_in_dim(sink, lax.axis_index("h") * att, att).reshape(kv, group)
    att_out, logs = attend(
        att_query.reshape(rows, kv, group, HEAD_DIM), att_key, att_value, logits, offset, total_rows
    )
    ret_out = retain(ret_query, ret_key, ret_value, decay)

    out_wide = gather(out_own, "t", 0)
    mixers = jnp.concatenate([att_out, ret_out], axis=1)
    if fused:
        sent = jnp.moveaxis(logs.reshape(att, parts, own), 1, 0)
        mixed, seen = back(mixers, out_wide, sent)
        return mixed, seen.reshape(parts * att, own)
    depth = out_wide.shape[1]
    out_wide = jnp.moveaxis(out_wide, 0, 1).reshape(depth, -1)
    mixed = jnp.dot(mixers, out_wide, preferred_element_type=jnp.float32).astype(jnp.bfloat16)
    mixed = lax.psum_scatter(mixed, ("h", "tp"), scatter_dimension=0, tiled=True)
    return mixed, exchange(logs, "h", 1, 0)


def solution(mesh):
    sp, tp = mesh.shape["sp"], mesh.shape["tp"]

    def run(*args):
        heads = math.gcd(args[3].shape[1], args[5].shape[1]) // HEAD_DIM
        parts = math.gcd(heads // math.gcd(heads, tp), sp)
        fine = Mesh(mesh.devices.reshape(sp // parts, parts, tp), ("t", "h", "tp"))
        seq = ("t", "h")
        body = jax.shard_map(
            shards,
            mesh=fine,
            in_specs=(P(seq, "tp"), P("tp"))
            + (P(seq, "tp"),) * 6
            + (P("tp", seq), P("tp", seq), P("tp"), P("tp", seq)),
            out_specs=(P(("t", "h", "tp"), None), P("tp", seq)),
            check_vma=False,
        )
        return body(*args)

    return run
```

profile of v0, /device:TPU:0, one launch (start us, length us, event | category | flops | bytes accessed | tf_op | source)
XLA Modules:
  0.0 308.4 jit_solution(16821674189623965535)
XLA Ops:
  7.2 1.5 copy.90
  8.8 1.7 fusion.9
  10.5 1.3 copy.91
  11.8 0.2 copy.78
  12.0 0.2 copy.84
  12.2 0.9 constant_dynamic-update-slice_fusion.5
  13.2 0.2 copy.85
  13.6 0.2 copy.86
  13.8 0.1 copy.81
  13.9 0.2 copy.87
  14.2 0.2 copy.88
  14.5 0.2 copy.89
  14.7 0.6 reshape.720.decay
  15.3 0.8 constant_dynamic-update-slice_fusion.4
  16.1 0.8 constant_dynamic-update-slice_fusion.3
  16.8 0.7 constant_dynamic-update-slice_fusion.2
  17.6 0.8 constant_dynamic-update-slice_fusion.1
  18.3 0.8 constant_dynamic-update-slice_fusion
  19.1 1.0 pad_maximum_fusion.1.outp
  20.1 135.4 %shard_map.131 = (f32[1024,896]{1,0:T(8,128)}, bf16[4,384,256]{2,1,0:T(8,128)(2,1)}, f32[4,2,2,128]{3,2,1,0:T(2,128)}, f32[4,1,256]{2,1,0:T(1,128)}) custom-call(bf16[4,256,896]{2,1,0:T(8,128)(2,1)} %bitcast.167, bf16[8,256,256]{2,1,0:T(8,128)(2,1)} %bitcast.159, f32[2,128]{1,0:T(2,128)} %bitcast.174, bf16[4,384,256]{2,1,0:T(8,128)(2,1)} %pad_maximum_fusion.1.outp, ...), custom_call_target="tpu_custom_call" | custom-call | flops 99999997952 | bytes 20000000 | tf_op jit(solution)/shard_map/pallas_call | solution.py:288
  155.5 0.7 reduce_sum.75
  156.3 2.0 multiply_bitcast_fusion
  158.3 2.4 fusion.50
  160.8 0.2 fusion.71
  160.9 1.3 collective-permute-start
  162.2 0.2 pad_maximum_fusion.3
  162.4 1.3 collective-permute-start.1
  163.8 0.3 reduce-window.6
  164.1 0.2 slice_reduce_fusion
  164.3 0.2 reduce-window.9
  164.6 0.6 slice.109
  165.2 0.6 slice.108
  167.1 0.8 convolution_bitcast_fusion.2
  167.9 0.7 convolution_bitcast_fusion.3
  168.7 26.0 %all-gather = f32[4,264,128]{2,1,0:T(8,128)S(1)} all-gather(f32[1,264,128]{2,1,0:T(8,128)S(1)} %maximum_maximum_fusion), channel_id=2, replica_groups=mesh['t'=4,'h'=4,'tp'=2] {'t'}, dimensions={0}, use_global_device_ids=true | all-gather | bytes 675840 | tf_op jit(solution)/shard_map/all_gather | solution.py:480
  194.9 0.2 select_reduce_fusion
  195.1 0.7 fusion.61
  195.9 0.4 fusion.28
  196.3 2.8 fusion.19
  199.0 0.5 fusion.60
  199.6 2.3 slice.86
  201.9 1.6 copy.113
  203.4 0.4 multiply_reduce_fusion
  203.9 1.0 multiply_cosine_fusion.1
  204.9 0.3 fusion.42
  205.2 0.1 broadcast_multiply_fusion
  205.4 0.2 subtract_convert_fusion
  205.5 1.0 fusion.14
  206.6 0.2 concatenate.53
  206.8 0.3 copy.97
  207.1 0.2 concatenate.54
  207.3 1.1 copy.98
  208.6 0.1 pad_maximum_fusion
  208.8 0.6 copy-done.1
  209.4 1.0 fusion.7
  210.5 1.0 fusion.6
  211.5 1.3 fusion.22
  212.8 0.4 copy.101
  213.3 1.0 pad_maximum_fusion.2.mixers
  214.3 0.7 fusion.53.logs
  215.0 22.8 %all-gather.3.cloned.1.call-done.wide = bf16[16,384,256]{2,1,0:T(8,128)(2,1)} async-done(((bf16[4,384,256]{2,1,0:T(8,128)(2,1)}), bf16[16,384,256]{2,1,0:T(8,128)(2,1)}) %all-gather.3.cloned.1.call-update) | async-done | bytes 3145744 | tf_op jit(solution)/shard_map/all_gather | solution.py:22
  237.7 60.2 %shard_map.132 = (bf16[128,4096]{1,0:T(8,128)(2,1)}, f32[4,2,256]{2,1,0:T(2,128)}) custom-call(bf16[1024,384]{1,0:T(8,128)(2,1)} %pad_maximum_fusion.2.mixers, bf16[16,384,256]{2,1,0:T(8,128)(2,1)} %all-gather.3.cloned.1.call-done.wide, f32[4,2,256]{2,1,0:T(2,128)} %fusion.53.logs), custom_call_target="tpu_custom_call" | custom-call | flops 49999998976 | bytes 20000000 | tf_op jit(solution)/shard_map/pallas_call | solution.py:413
  297.9 1.3 reshape.734
  299.2 2.3 copy.123
  (60 shorter events, 1.9 us)
Async XLA Ops:
  7.2 4.6 %copy-start.2 = (bf16[256,1024]{1,0:T(8,128)(2,1)S(1)}, bf16[256,1024]{1,0:T(8,128)(2,1)}, u32[]{:S(2)}) copy-start(bf16[256,1024]{1,0:T(8,128)(2,1)} %param.14) | copy-start | bytes 1572868
  7.2 230.6 %all-gather.3.cloned.1.call-start = ((), (), s32[]{:S(2)}) async-start(), calls=%async_computation | async-start | bytes 3932160 | tf_op jit(solution)/shard_map/all_gather | solution.py:22
  8.8 4.3 %copy-start.3 = (bf16[256,512]{1,0:T(8,128)(2,1)S(1)}, bf16[256,512]{1,0:T(8,128)(2,1)}, u32[]{:S(2)}) copy-start(bf16[256,512]{1,0:T(8,128)(2,1)} %param.15) | copy-start | bytes 786436
  10.5 2.9 copy-start.4
  10.5 3.3 %copy-start.5 = (bf16[256,512]{1,0:T(8,128)(2,1)S(1)}, bf16[256,512]{1,0:T(8,128)(2,1)}, u32[]{:S(2)}) copy-start(bf16[256,512]{1,0:T(8,128)(2,1)} %param.17) | copy-start | bytes 786436
  11.8 2.3 copy-start.6
  11.8 2.6 copy-start.7
  12.0 2.7 copy-start.9
  13.2 5.9 %copy-start = (bf16[1024,256]{1,0:T(8,128)(2,1)S(1)}, bf16[1024,256]{1,0:T(8,128)(2,1)}, u32[]{:S(2)}) copy-start(bf16[1024,256]{1,0:T(8,128)(2,1)} %param.20) | copy-start | bytes 1572868
  13.2 5.9 %copy-start.8 = (bf16[512,256]{1,0:T(8,128)(2,1)S(1)}, bf16[512,256]{1,0:T(8,128)(2,1)}, u32[]{:S(2)}) copy-start(bf16[512,256]{1,0:T(8,128)(2,1)} %param.21) | copy-start | bytes 786436
  158.3 5.5 %copy-start.10 = (f32[4,1,256]{2,1,0:T(1,128)S(1)}, f32[4,1,256]{2,1,0:T(1,128)}, u32[]{:S(2)}) copy-start(f32[4,1,256]{2,1,0:T(1,128)} %get-tuple-element.10) | copy-start | bytes 12292
  160.9 47.6 %collective-permute-start = (bf16[2,128,1,128]{3,1,0,2:T(8,128)(2,1)S(1)}, bf16[2,128,1,128]{3,1,0,2:T(8,128)(2,1)S(1)}, u32[]{:S(2)}, u32[]{:S(2)}) collective-permute-start(bf16[2,128,1,128]{3,1,0,2:T(8,128)(2,1)S(1)} %slice.100), channel_id=1, source_target_pairs={{0,8},{8,16},{16,24},{1,9},{9,17},{17,25},{2,10},{10,18},{18,26},{... | collective-permute-start | bytes 196616 | tf_op jit(solution)/shard_map/ppermute | solution.py:35
  162.4 46.0 %collective-permute-start.1 = (bf16[2,128,1,128]{3,1,2,0:T(8,128)(2,1)S(1)}, bf16[2,128,1,128]{3,1,2,0:T(8,128)(2,1)S(1)}, u32[]{:S(2)}, u32[]{:S(2)}) collective-permute-start(bf16[2,128,1,128]{3,1,2,0:T(8,128)(2,1)S(1)} %slice.103), channel_id=1, source_target_pairs={{8,0},{16,8},{24,16},{9,1},{17,9},{25,17},{10,2},{18,10},{26,18},{... | collective-permute-start | bytes 196616 | tf_op jit(solution)/shard_map/ppermute | solution.py:36
  205.2 3.1 %copy-start.11 = (f32[8]{0:T(128)S(1)}, f32[8]{0:T(128)}, u32[]{:S(2)}) copy-start(f32[8]{0:T(128)} %param.22) | copy-start | bytes 100
  208.3 1.0 copy-start.1
Sparse Core Ops, SparseCore 0:
  163.9 73.8 all-gather.2
where the time goes:
time: 310 us; the launch traced here: 308 us
  Pallas kernels  196 us (63%)
  blocking collectives  26 us (8%)
  waiting for transfers between devices  22.8 us (7%)
  local copies, waits for them, and re-layouts  22 us (7%)
  between operations  15.8 us (5%)
  other arithmetic  15.5 us (5%)
  matrix products  8.1 us (3%)
    pallas_call x1, Pallas kernels, front(): pl.pallas_call(functools.partial(front_kernel, peers, parts, cores), out_...  135 us
    pallas_call x1, Pallas kernels, back(): pl.pallas_call(functools.partial(back_kernel, parts, cores), out_shape=(j...  60.2 us
    all_gather x1, blocking collectives, retain(): seen = lax.all_gather(sent, 't', axis=0)  26 us
    all_gather x1, waiting for transfers between devices, gather(): return lax.all_gather(x, axis, axis=dim, tiled=True)  22.8 us
    unnamed x38, local copies, waits for them, and re-layouts  9.29 us
  transfers between devices with their start and end apart: 3, of which 1 were waited for; matrix products, arithmetic and copies ran while one was open for 8% of the time, Pallas kernels for 0%

commit v1 on v0

v1 whole, which is shorter than its diff:
```python
import math

import jax
import jax.numpy as jnp
import numpy as np
from jax import lax
from jax.experimental import pallas as pl
from jax.experimental.pallas import tpu as pltpu
from jax.sharding import Mesh
from jax.sharding import PartitionSpec as P

HEAD_DIM = 128
SPAN_RADIUS = 128
BLOCK = 256
HIGHEST = lax.Precision.HIGHEST
MESH = pl.DeviceIdType.MESH


def gather(x, axis, dim):
    if lax.axis_size(axis) == 1:
        return x
    return lax.all_gather(x, axis, axis=dim, tiled=True)


def exchange(x, axis, split, concat):
    if lax.axis_size(axis) == 1:
        return x
    return lax.all_to_all(x, axis, split, concat, tiled=True)


def halo(shard, axis, width):
    peers, length = lax.axis_size(axis), shard.shape[1]
    up = [(i, i + 1) for i in range(peers - 1)]
    down = [(j, i) for i, j in up]
    before = lax.ppermute(shard[:, length - width :], axis, up)
    after = lax.ppermute(shard[:, :width], axis, down)
    return jnp.concatenate([before, shard, after], axis=1)


def rotate(values, cosine, sine):
    half = values.shape[-1] // 2
    first, second = values[..., :half], values[..., half:]
    return jnp.concatenate(
        [first * cosine - second * sine, second * cosine + first * sine], axis=-1
    ).astype(jnp.bfloat16)


class Stream:
    def __init__(self, where, remote, refs, pack):
        self.where, self.remote, self.pack = where, remote, pack
        (
            self.wide, self.away, self.out,
            self.load, self.x_send, self.z_send, self.h_send, self.y_send,
            self.p_recv, self.w_recv,
        ) = refs

    def fetch(self):
        w = self.where
        targets = (
            (self.out.at[0], 1 - w.g, 1 - w.x),
            (self.out.at[1], w.g, 1 - w.x),
            (self.wide.at[w.own], w.g, w.x),
            (self.away.at[w.x], 1 - w.g, w.x),
        )
        for i, (target, g, x) in enumerate(targets):
            self.pack(2 * g + x, target, self.load.at[i])

    def fetched(self):
        w = self.where
        for i, target in enumerate(
            (self.out.at[0], self.out.at[1], self.wide.at[w.own], self.away.at[w.x])
        ):
            pltpu.make_async_copy(target, target, self.load.at[i]).wait()

    def along_x(self, k):
        w = self.where
        if k == 0:
            return self.remote(
                self.out.at[0], self.away.at[w.x], self.x_send.at[0], self.p_recv.at[0], w.to_x
            )
        return self.remote(
            self.out.at[1], self.wide.at[w.own], self.x_send.at[1], self.w_recv.at[w.own], w.to_x
        )

    def along_z(self, k):
        w = self.where
        x = w.x if k == 0 else 1 - w.x
        s = w.at(w.zh, w.zl, w.y, x)
        return self.remote(
            self.away.at[x], self.wide.at[s], self.z_send.at[k], self.w_recv.at[s], w.to_z
        )

    def near(self, k):
        w = self.where
        return w.at(w.zh, (w.zl, 1 - w.zl)[k // 2], w.y, (w.x, 1 - w.x)[k % 2])

    def far(self, k):
        w = self.where
        return w.at(1 - w.zh, (w.zl, 1 - w.zl)[1 - k // 2], w.y, (w.x, 1 - w.x)[k % 2])

    def along_h(self, k):
        s = self.near(k)
        return self.remote(
            self.wide.at[s], self.wide.at[s], self.h_send.at[k], self.w_recv.at[s], self.where.to_h
        )

    def along_y(self, k):
        s = self.near(k) if k < 4 else self.far(k - 4)
        return self.remote(
            self.wide.at[s], self.wide.at[s], self.y_send.at[k], self.w_recv.at[s], self.where.to_y
        )

    def arrive(self, s):
        self.remote(
            self.wide.at[s], self.wide.at[s], self.x_send.at[0], self.w_recv.at[s], self.where.to_x
        ).wait_recv()

    def arrive_away(self):
        w = self.where
        slot = self.away.at[1 - w.x]
        self.remote(slot, slot, self.x_send.at[0], self.p_recv.at[0], w.to_x).wait_recv()

    def arrive_across(self):
        w = self.where
        for zh in (w.zh, 1 - w.zh):
            for zl in range(2):
                for x in range(2):
                    self.arrive(w.at(zh, zl, 1 - w.y, x))

    def drain(self):
        for k in range(2):
            self.along_x(k).wait_send()
            self.along_z(k).wait_send()
        for k in range(4):
            self.along_h(k).wait_send()
        for k in range(8):
            self.along_y(k).wait_send()


class Place:
    def __init__(self):
        self.zh, self.zl, self.y, self.x, self.c = (
            lax.axis_index(a) for a in ("zh", "zl", "y", "x", "tp")
        )
        self.g = lax.rem(self.zh + self.zl, 2)
        self.h = 2 * self.g + self.x
        self.own = self.at(self.zh, self.zl, self.y, self.x)
        self.b = 2 * self.zl + self.x
        self.to_x = {"x": 1 - self.x}
        self.to_z = {"zl": 1 - self.zl}
        self.to_y = {"y": 1 - self.y}
        self.to_h = {"zh": 1 - self.zh, "zl": 1 - self.zl}
        self.to_hy = {"zh": 1 - self.zh, "zl": 1 - self.zl, "y": 1 - self.y}
        self.to_zx = {"zl": 1 - self.zl, "x": 1 - self.x}
        self.to_c = {"tp": 1 - self.c}

    @staticmethod
    def at(zh, zl, y, x):
        return ((zh * 2 + zl) * 2 + y) * 2 + x


def fused_kernel(
    tokens, gain, q_att, k_att, v_att, q_ret, k_ret, v_ret, out_att, out_ret, sink, decay,
    cos_t, sin_t, base,
    mixed, logs_out,
    raw, scl, ssq, gains, proj, kvext, qrot, rets, dec, cumr, cumc, coef, states, stall,
    mix, logm, lsend, lrecv, mine, give, take, s1, r1, s2, r2,
    t_load, t_x, t_z, t_c, t_recv, g_sem, d_sem, halo_sem, st_sem, l_sem,
    give_s, take_r, s1_s, r1_r, s2_s, r2_r,
    *streams,
):
    w = Place()
    f32, bf16 = jnp.float32, jnp.bfloat16
    own, half_d = tokens.shape
    rows = 4 * own
    run_rows = 2 * own
    total_rows = 16 * own
    H = HEAD_DIM
    edge = SPAN_RADIUS

    def remote(src, dst, send, recv, to):
        return pltpu.make_async_remote_copy(
            src_ref=src, dst_ref=dst, send_sem=send, recv_sem=recv,
            device_id=to, device_id_type=MESH,
        )

    def lanes(h, n):
        return pl.ds(pl.multiple_of(h * n, n), n)

    def pack_cols(parts):
        def pack(h, target, sem):
            start = 0
            for ref in parts:
                n = ref.shape[1] // 4
                pltpu.make_async_copy(
                    ref.at[:, lanes(h, n)], target.at[:, pl.ds(start, n)], sem
                ).start()
                start += n
        return pack

    def pack_rows(parts):
        def pack(h, target, sem):
            start = 0
            for ref in parts:
                n = ref.shape[0] // 4
                pltpu.make_async_copy(
                    ref.at[lanes(h, n), :], target.at[pl.ds(start, n), :], sem
                ).start()
                start += n
        return pack

    n = len(streams) // 3
    A = Stream(w, remote, streams[:n], pack_cols((q_att, k_att, v_att)))
    R = Stream(w, remote, streams[n : 2 * n], pack_cols((q_ret, k_ret, v_ret)))
    O = Stream(w, remote, streams[2 * n :], pack_rows((out_att, out_ret)))

    token_load = pltpu.make_async_copy(tokens, raw.at[w.c, w.b], t_load.at[0])
    gain_load = pltpu.make_async_copy(gain, gains.at[w.c], t_load.at[1])
    decay_load = pltpu.make_async_copy(decay, dec.at[w.zh, w.y, w.zl, w.x], t_load.at[2])

    def block(zl, x):
        return 2 * zl + x

    def token(b, send, to):
        here = raw.at[w.c, b]
        return remote(here, here, send, t_recv.at[w.c, b], to)

    tokens_x = (
        token(w.b, t_x.at[0], w.to_x),
        token(block(1 - w.zl, w.x), t_x.at[1], w.to_x),
    )
    tokens_z = token(w.b, t_z.at[0], w.to_z)

    def tokens_c(k):
        b = block((w.zl, 1 - w.zl)[k // 2], (w.x, 1 - w.x)[k % 2])
        return token(b, t_c.at[k], w.to_c)

    def token_arrive(k, e=None):
        b = block((w.zl, 1 - w.zl)[k // 2], (w.x, 1 - w.x)[k % 2])
        e = w.c if e is None else e
        here = raw.at[e, b]
        remote(here, here, t_x.at[0], t_recv.at[e, b], w.to_x).wait_recv()

    gain_c = remote(gains.at[w.c], gains.at[w.c], g_sem.at[0], g_sem.at[1], w.to_c)

    d_parts = (
        (dec.at[w.zh, w.y, w.zl, w.x], dec.at[w.zh, w.y, w.zl, 1 - w.x], w.to_x),
        (dec.at[w.zh, w.y, w.zl], dec.at[w.zh, w.y, 1 - w.zl], w.to_z),
        (dec.at[w.zh, w.y], dec.at[w.zh, 1 - w.y], w.to_y),
        (dec.at[w.zh], dec.at[1 - w.zh], w.to_h),
    )

    def decay_send(k):
        src, _, to = d_parts[k]
        return remote(src, src, d_sem.at[0, k], d_sem.at[1, k], to)

    def decay_arrive(k):
        _, dst, to = d_parts[k]
        remote(dst, dst, d_sem.at[0, k], d_sem.at[1, k], to).wait_recv()

    A.fetch()
    token_load.start()
    gain_load.start()
    decay_load.start()
    R.fetch()
    O.fetch()

    barrier = pltpu.get_barrier_semaphore()
    friends = (w.to_x, w.to_z, w.to_y, w.to_h, w.to_hy, w.to_zx, w.to_c)
    for to in friends:
        pl.semaphore_signal(barrier, inc=1, device_id=to, device_id_type=MESH)
    pl.semaphore_wait(barrier, len(friends))

    middle = w.g == 1

    A.fetched()
    A.along_x(0).start()
    A.along_z(0).start()
    A.along_y(0).start()
    R.fetched()
    R.along_x(0).start()
    R.along_z(0).start()
    R.along_y(0).start()
    A.along_x(1).start()
    R.along_x(1).start()

    @pl.when(middle)
    def _():
        A.along_h(0).start()
        R.along_h(0).start()

    decay_load.wait()
    gain_load.wait()
    gain_c.start()
    decay_send(0).start()
    token_load.wait()
    tokens_x[0].start()
    tokens_c(0).start()

    def scale(e, b):
        @pl.loop(0, own // 16)
        def _(i):
            value = raw[e, b, pl.ds(pl.multiple_of(i * 16, 16), 16), :].astype(f32)
            at = pl.ds(pl.multiple_of(b * own + i * 16, 16), 16)
            scl[e, at, :] = (value * gains[e]).astype(bf16)
            square = value * value
            total = square[:, :H]
            for k in range(1, half_d // H):
                total = total + square[:, k * H : (k + 1) * H]
            ssq[e, at, :] = total

    @pl.when((w.zh == 0) & (w.y == 0))
    def _():
        kvext[0, :, 0:edge, :] = jnp.zeros((2, edge, H), bf16)

    @pl.when((w.zh == 1) & (w.y == 1))
    def _():
        kvext[1, :, edge + run_rows :, :] = jnp.zeros((2, edge, H), bf16)

    scale(w.c, w.b)
    A.arrive_away()
    A.along_z(1).start()
    decay_arrive(0)
    decay_send(1).start()
    R.arrive_away()
    R.along_z(1).start()
    tokens_z.start()
    decay_arrive(1)
    decay_send(2).start()
    remote(gains.at[1 - w.c], gains.at[1 - w.c], g_sem.at[0], g_sem.at[1], w.to_c).wait_recv()
    token_arrive(0, 1 - w.c)
    scale(1 - w.c, w.b)
    for k in (2, 1, 3):
        for stream in (A, R):
            stream.arrive(stream.near(k))
            stream.along_y(k).start()

            @pl.when(middle)
            def _():
                stream.along_h(k).start()

    @pl.when(w.g == 0)
    def _():
        for k in range(4):
            A.along_h(k).start()
        for k in range(4):
            R.along_h(k).start()

    decay_arrive(2)
    decay_send(3).start()
    decay_arrive(3)

    lane = lax.broadcasted_iota(jnp.int32, (8, run_rows), 1)
    for slot in range(2):
        row = jnp.concatenate(
            [dec[w.zh, w.y, slot, x, pl.ds(w.h, 1), :] for x in range(2)], axis=1
        )
        row = jnp.broadcast_to(row, (8, run_rows))
        step = 1
        while step < run_rows:
            row = row + jnp.where(lane >= step, pltpu.roll(row, step, axis=1), 0.0)
            step *= 2
        cumr[slot] = row
        cumc[slot] = jnp.transpose(jnp.broadcast_to(row[0:1], (H, run_rows)))
    lane = lax.broadcasted_iota(jnp.int32, (8, H), 1)
    run = lax.broadcasted_iota(jnp.int32, (8, H), 0)
    totals = jnp.zeros((8, H), f32)
    for zh in range(2):
        for slot in range(2):
            for y in range(2):
                pair = sum(dec[zh, y, slot, x, pl.ds(w.h, 1), :] for x in range(2))
                value = jnp.sum(pair, axis=1, keepdims=True)
                totals = jnp.where(lane == 4 * zh + 2 * slot + y, value, totals)
    for slot in range(2):
        me = 4 * w.zh + 2 * slot + w.y
        between = (lane > jnp.minimum(run, me)) & (lane < jnp.maximum(run, me))
        factor = jnp.exp(jnp.sum(jnp.where(between, totals, 0.0), axis=1, keepdims=True))
        factor = jnp.broadcast_to(factor, (8, H))
        coef[slot, 0] = jnp.where(run < me, factor, 0.0)
        coef[slot, 1] = jnp.where(run > me, factor, 0.0)

    token_arrive(2)
    tokens_x[1].start()
    tokens_c(2).start()
    token_arrive(1)
    tokens_c(1).start()
    O.fetched()
    O.along_x(0).start()
    O.along_x(1).start()
    for k in (2, 1):
        b = block((w.zl, 1 - w.zl)[k // 2], (w.x, 1 - w.x)[k % 2])
        scale(w.c, b)
    for k in (2, 1):
        b = block((w.zl, 1 - w.zl)[k // 2], (w.x, 1 - w.x)[k % 2])
        token_arrive(k, 1 - w.c)
        scale(1 - w.c, b)
    for k in range(4):
        A.arrive(A.far(k))
        A.along_y(4 + k).start()

    def pass_far(stream, k):
        stream.arrive(stream.far(k))
        stream.along_y(4 + k).start()

    @pl.when(middle)
    def _():
        for k in range(4):
            pass_far(R, k)

    token_arrive(3)
    tokens_c(3).start()
    b3 = block(1 - w.zl, 1 - w.x)
    scale(w.c, b3)
    token_arrive(3, 1 - w.c)
    scale(1 - w.c, b3)
    O.along_z(0).start()
    A.arrive_across()

    def project(stream, b, start, width):
        at = pl.ds(pl.multiple_of(b * own, own), own)
        depth = half_d // own
        first = stream.wide[0:depth, :, start : start + width].reshape(half_d, width)
        second = stream.wide[depth : 2 * depth, :, start : start + width].reshape(half_d, width)
        value = jnp.dot(scl[0, at, :], first, preferred_element_type=f32)
        return value + jnp.dot(scl[1, at, :], second, preferred_element_type=f32)

    def inverse(b):
        at = pl.ds(pl.multiple_of(b * own, own), own)
        squares = jnp.sum(ssq[0, at, :] + ssq[1, at, :], axis=1, keepdims=True)
        return lax.rsqrt(squares / (2 * half_d) + 1e-06)

    def angles(b):
        s = w.at(w.zh, b // 2, w.y, b % 2)
        c0, s0, s0n, c0n = (base[i, pl.ds(s, 1), :] for i in range(4))
        cosine = cos_t[...] * c0 - sin_t[...] * s0
        sine = cos_t[...] * s0n + sin_t[...] * c0n
        return cosine, sine

    def turn(value, cosine, sine):
        return (value * cosine + pltpu.roll(value, H // 2, axis=1) * sine).astype(bf16)

    def attention_inputs(b):
        at = pl.ds(pl.multiple_of(b * own, own), own)
        scale_b = inverse(b)
        cosine, sine = angles(b)
        query = project(A, b, 0, 2 * H) * scale_b
        qrot[at, :H] = turn(query[:, :H], cosine, sine)
        qrot[at, H:] = turn(query[:, H:], cosine, sine)
        other = project(A, b, 2 * H, 2 * H) * scale_b
        inner = pl.ds(pl.multiple_of(edge + (b % 2) * own, edge), own)
        kvext[b // 2, 0, inner, :] = turn(other[:, :H], cosine, sine)
        kvext[b // 2, 1, inner, :] = other[:, H:].astype(bf16)

    @pl.loop(0, 4)
    def _(b):
        attention_inputs(b)

    y = w.y
    head, tail, before_at, after_at = edge, run_rows, 0, edge + run_rows

    def pick(a, b):
        return a + (b - a) * y

    def piece(slot, start):
        return kvext.at[slot, :, pl.ds(pl.multiple_of(start, edge), edge), :]

    halo_y = [
        remote(
            piece(pick(s0, s1), pick(f0, f1)), piece(pick(d0, d1), pick(o0, o1)),
            halo_sem.at[0, i], halo_sem.at[1, i], w.to_y,
        )
        for i, (s0, f0, d0, o0, s1, f1, d1, o1) in enumerate(
            (
                (0, tail, 0, before_at, 0, head, 0, after_at),
                (1, head, 0, after_at, 0, tail, 1, before_at),
                (1, tail, 1, before_at, 1, head, 1, after_at),
            )
        )
    ]
    halo_far = remote(
        piece(pick(0, 1), pick(head, tail)), piece(pick(1, 0), pick(after_at, before_at)),
        halo_sem.at[0, 3], halo_sem.at[1, 3], w.to_hy,
    )
    has_far = ((y == 0) & (w.zh == 1)) | ((y == 1) & (w.zh == 0))
    for copy in halo_y:
        copy.start()

    @pl.when(has_far)
    def _():
        halo_far.start()

    @pl.when(w.g == 0)
    def _():
        for k in range(4):
            pass_far(R, k)

    O.along_y(0).start()
    O.along_h(0).start()
    O.arrive_away()
    O.along_z(1).start()

    def halo_arrive(slot, start, i, to):
        here = piece(slot, start)
        remote(here, here, halo_sem.at[0, i], halo_sem.at[1, i], to).wait_recv()

    halo_arrive(pick(0, 0), pick(after_at, before_at), 0, w.to_y)
    halo_arrive(pick(1, 0), pick(before_at, after_at), 1, w.to_y)
    halo_arrive(pick(1, 1), pick(after_at, before_at), 2, w.to_y)

    @pl.when(has_far)
    def _():
        halo_arrive(pick(0, 1), pick(before_at, after_at), 3, w.to_hy)

    def attend_tile(i):
        slot, j = i // 4, i % 4
        query = qrot[pl.ds(pl.multiple_of(i * edge, edge), edge), :]
        query = jnp.concatenate([query[:, :H], query[:, H:]], axis=0)
        span = pl.ds(pl.multiple_of(j * edge, edge), 3 * edge)
        key, value = kvext[slot, 0, span, :], kvext[slot, 1, span, :]
        score = lax.dot_general(
            query, key, (((1,), (1,)), ((), ())), preferred_element_type=f32
        ) * H ** (-0.5)
        row = lax.broadcasted_iota(jnp.int32, score.shape, 0)
        col = lax.broadcasted_iota(jnp.int32, score.shape, 1)
        shift = col - jnp.where(row < edge, row, row - edge)
        start = w.at(w.zh, slot, y, 0) * own + j * edge - edge
        valid = (
            (shift >= 0) & (shift <= 2 * edge) & (col >= -start) & (col < total_rows - start)
        )
        masked = jnp.where(valid, score, -jnp.inf)
        first = lax.broadcasted_iota(jnp.int32, (2 * edge, 1), 0) < edge
        limit = jnp.where(first, sink[2 * w.h], sink[2 * w.h + 1])
        top = jnp.maximum(jnp.max(masked, axis=1, keepdims=True), limit)
        expo = jnp.exp(masked - top)
        total = jnp.sum(expo, axis=1, keepdims=True) + jnp.exp(limit - top)
        logs = top + jnp.log(total)
        probs = (expo * (1.0 / total)).astype(bf16)
        result = jnp.dot(probs, value, preferred_element_type=f32).astype(bf16)
        at = pl.ds(pl.multiple_of((i // 2) * edge, edge), edge)
        mix[i % 2, at, 0:H] = result[:edge]
        mix[i % 2, at, H : 2 * H] = result[edge:]
        column = lax.broadcasted_iota(jnp.int32, (2 * edge, H), 1)
        logm[...] = jnp.where(column == i, logs, logm[...])

    logm[...] = jnp.zeros_like(logm)

    @pl.loop(0, 4)
    def _(i):
        attend_tile(i)

    for k in (2, 1, 3):
        O.arrive(O.near(k))
        O.along_y(k).start()

        @pl.when(middle)
        def _():
            O.along_h(k).start()

    @pl.loop(4, 8)
    def _(i):
        attend_tile(i)

    turned = jnp.transpose(logm[...])
    for b in range(4):
        lsend[b] = turned[2 * b : 2 * b + 2]
        lrecv[w.h] = jnp.where(w.b == b, turned[2 * b : 2 * b + 2], lrecv[w.h] if b else 0.0)
    h_of = lambda zl, x: 2 * lax.rem(w.zh + zl, 2) + x
    log_to = (
        (1 - w.x, w.zl, w.to_x), (w.x, 1 - w.zl, w.to_z), (1 - w.x, 1 - w.zl, w.to_zx),
    )
    log_sends = [
        remote(lsend.at[block(zl, x)], lrecv.at[w.h], l_sem.at[0, i], l_sem.at[1, i], to)
        for i, (x, zl, to) in enumerate(log_to)
    ]

    R.arrive_across()

    def retention_inputs(b):
        at = pl.ds(pl.multiple_of(b * own, own), own)
        scale_b = inverse(b)
        both = project(R, b, 0, 2 * H)
        rets[0, at, :] = (both[:, :H] * scale_b).astype(bf16)
        rets[1, at, :] = (both[:, H:] * (scale_b * H ** (-0.5))).astype(bf16)
        rets[2, at, :] = (project(R, b, 2 * H, H) * scale_b).astype(bf16)

    @pl.loop(0, 4)
    def _(b):
        retention_inputs(b)

    for slot in range(2):
        at = pl.ds(slot * run_rows, run_rows)
        last = cumr[slot, 0:1, run_rows - 1 : run_rows]
        key, value = rets[1, at, :].astype(f32), rets[2, at, :]
        for i, weight in enumerate((jnp.exp(last - cumc[slot]), jnp.exp(cumc[slot]))):
            lhs = (key * weight).astype(bf16)
            state = lax.dot_general(
                lhs, value, (((0,), (0,)), ((), ())), preferred_element_type=f32
            ).astype(bf16)
            stall[w.zh, w.y, slot, i] = state
    state_sends = [
        remote(
            stall.at[w.zh, w.y], stall.at[w.zh, w.y], st_sem.at[0, i], st_sem.at[1, i], to
        )
        for i, to in enumerate((w.to_y, w.to_h, w.to_hy))
    ]
    for copy in state_sends:
        copy.start()
    for copy in log_sends:
        copy.start()

    @pl.when(w.g == 0)
    def _():
        for k in range(1, 4):
            O.along_h(k).start()

    def inner_tile(i):
        slot = i // 2
        at = pl.ds(pl.multiple_of(i * own, own), own)
        keys = pl.ds(pl.multiple_of(slot * run_rows, run_rows), run_rows)
        score = lax.dot_general(
            rets[0, at, :], rets[1, keys, :], (((1,), (1,)), ((), ())),
            preferred_element_type=f32,
        )
        column = cumc[slot, pl.ds(pl.multiple_of((i % 2) * own, own), own), :]
        column = jnp.concatenate([column] * (run_rows // H), axis=1)
        weight = jnp.exp(-jnp.abs(column - cumr[slot, 0:1, :]))
        proj[at, :] = jnp.dot(
            (score * weight).astype(bf16), rets[2, keys, :], preferred_element_type=f32
        )

    @pl.loop(0, 4)
    def _(i):
        inner_tile(i)

    for i, (zh, yy) in enumerate(((w.zh, 1 - y), (1 - w.zh, y), (1 - w.zh, 1 - y))):
        here = stall.at[zh, yy]
        remote(here, here, st_sem.at[0, i], st_sem.at[1, i], w.to_y).wait_recv()
    for slot in range(2):
        for i in range(2):
            total = jnp.zeros((H, H), f32)
            for zh in range(2):
                for s in range(2):
                    for yy in range(2):
                        r = 4 * zh + 2 * s + yy
                        total = total + coef[slot, i, r : r + 1, :] * stall[
                            zh, yy, s, i
                        ].astype(f32)
            states[slot, :, i * H : (i + 1) * H] = total.astype(bf16)

    def finish_tile(i):
        slot = i // 2
        at = pl.ds(pl.multiple_of(i * own, own), own)
        column = cumc[slot, pl.ds(pl.multiple_of((i % 2) * own, own), own), :]
        last = cumr[slot, 0:1, run_rows - 1 : run_rows]
        carried = jnp.dot(rets[0, at, :], states[slot], preferred_element_type=f32)
        value = (
            proj[at, :] + jnp.exp(column) * carried[:, :H]
            + jnp.exp(last - column) * carried[:, H:]
        )
        value = value - jnp.mean(value, axis=1, keepdims=True)
        value = value * lax.rsqrt(jnp.mean(value * value, axis=1, keepdims=True) + 1e-06)
        value = value.astype(bf16)
        out = pl.ds(pl.multiple_of(i * edge, edge), edge)
        mix[0, out, 2 * H :] = value[:edge]
        mix[1, out, 2 * H :] = value[edge:]

    @pl.loop(0, 4)
    def _(i):
        finish_tile(i)

    for k in range(4):
        pass_far(O, k)

    chunks = 8

    def columns_of(i, x):
        a, far, zl = i // 4, (i // 2) % 2, i % 2
        yy = a + y - 2 * a * y
        zh = far + w.zh - 2 * far * w.zh
        return w.at(zh, zl, yy, x)

    def swap(i):
        return remote(give.at[i], take.at[i], give_s.at[i], take_r.at[i], w.to_c)

    def first_hop(i):
        return (
            remote(s1.at[i, 0], r1.at[i, 0], s1_s.at[i, 0], r1_r.at[i, 0], w.to_x),
            remote(s1.at[i, 1], r1.at[i, 1], s1_s.at[i, 1], r1_r.at[i, 1], w.to_z),
        )

    def second_hop(i):
        return (
            remote(s2.at[i, 0], r2.at[i, 0], s2_s.at[i, 0], r2_r.at[i, 0], w.to_z),
            remote(s2.at[i, 1], r2.at[i, 1], s2_s.at[i, 1], r2_r.at[i, 1], w.to_x),
        )

    def part(b):
        return pl.ds(pl.multiple_of(b * edge, edge), edge)

    @pl.loop(0, chunks + 3)
    def _(step):
        @pl.when(step < chunks)
        def _():
            i = step

            @pl.when(i >= chunks // 2)
            def _():
                for x in range(2):
                    O.arrive(columns_of(i, x))

            for k in range(2):
                give[i, k] = jnp.dot(
                    mix[1 - w.c], O.wide[columns_of(i, k)], preferred_element_type=f32
                ).astype(bf16)
            swap(i).start()
            for k in range(2):
                mine[i, k] = jnp.dot(
                    mix[w.c], O.wide[columns_of(i, k)], preferred_element_type=f32
                )

        @pl.when((step >= 1) & (step < chunks + 1))
        def _():
            i = step - 1
            swap(i).wait_recv()
            for k in range(2):
                for j in range(2):
                    b = block(j, 1 - w.x) if k == 0 else block(1 - w.zl, j)
                    total = mine[i, k, part(b), :] + take[i, k, part(b), :].astype(f32)
                    s1[i, k, j] = total.astype(bf16)
            for copy in first_hop(i):
                copy.start()
            for k in range(2):
                for j in range(2):
                    b = block(j, w.x) if k == 0 else block(w.zl, j)
                    mine[i, k, part(b), :] += take[i, k, part(b), :].astype(f32)

        @pl.when((step >= 2) & (step < chunks + 2))
        def _():
            i = step - 2
            for k, copy in enumerate(first_hop(i)):
                copy.wait_recv()
                b = block(1 - w.zl, w.x) if k == 0 else block(w.zl, 1 - w.x)
                j = 1 - w.zl if k == 0 else 1 - w.x
                s2[i, k] = (mine[i, k, part(b), :] + r1[i, k, j].astype(f32)).astype(bf16)
                second_hop(i)[k].start()
            for k in range(2):
                j = w.zl if k == 0 else w.x
                mine[i, k, part(w.b), :] += r1[i, k, j].astype(f32)

        @pl.when(step >= 3)
        def _():
            i = step - 3
            for k, copy in enumerate(second_hop(i)):
                copy.wait_recv()
                at = pl.ds(pl.multiple_of(columns_of(i, k) * own, own), own)
                total = mine[i, k, part(w.b), :] + r2[i, k].astype(f32)
                mixed[:, at] = total.astype(mixed.dtype)

    for i, (x, zl, to) in enumerate(log_to):
        here = lrecv.at[h_of(zl, x)]
        remote(here, here, l_sem.at[0, i], l_sem.at[1, i], to).wait_recv()
    for h in range(4):
        for head_i in range(2):
            for t in range(2):
                logs_out[2 * h + head_i : 2 * h + head_i + 1, t * edge : (t + 1) * edge] = (
                    lrecv[h, t : t + 1, head_i * edge : (head_i + 1) * edge]
                )

    for stream in (A, R, O):
        stream.drain()
    for k in range(4):
        tokens_c(k).wait_send()
        decay_send(k).wait_send()
    for copy in tokens_x + (tokens_z, gain_c):
        copy.wait_send()
    for copy in halo_y + state_sends + log_sends:
        copy.wait_send()

    @pl.when(has_far)
    def _():
        halo_far.wait_send()

    @pl.loop(0, chunks)
    def _(i):
        swap(i).wait_send()
        for copy in first_hop(i) + second_hop(i):
            copy.wait_send()


def fused(*args):
    tokens, gain, q_att = args[:3]
    out_att, out_ret, sink, decay_log = args[8:]
    own, half_d = tokens.shape
    rows, run_rows = 4 * own, 2 * own
    H, edge = HEAD_DIM, SPAN_RADIUS
    bf16, f32 = jnp.bfloat16, jnp.float32
    dma, vmem = pltpu.SemaphoreType.DMA, pltpu.VMEM
    depth = q_att.shape[0]
    width = out_att.shape[1] * 16

    freqs = 10000.0 ** (-np.arange(0, H, 2, dtype=np.float64) / H)
    freqs = np.concatenate([freqs, freqs])[None, :]
    sign = np.where(np.arange(H) < H // 2, -1.0, 1.0)[None, :]
    inner = np.arange(own)[:, None] * freqs
    outer = (np.arange(16) * own)[:, None] * freqs
    cos_t, sin_t = jnp.asarray(np.cos(inner), f32), jnp.asarray(np.sin(inner), f32)
    base = jnp.asarray(
        np.stack([np.cos(outer), np.sin(outer), sign * np.sin(outer), sign * np.cos(outer)]), f32
    )

    def stream(block):
        return [
            vmem((16,) + block, bf16), vmem((2,) + block, bf16), vmem((2,) + block, bf16),
            dma((4,)), dma((2,)), dma((2,)), dma((4,)), dma((8,)), dma((1,)), dma((16,)),
        ]

    out_rows = (out_att.shape[0] + out_ret.shape[0]) // 4
    tile = (8, 2, 4 * edge, own)
    hbm, inside = pl.BlockSpec(memory_space=pl.ANY), pl.BlockSpec(memory_space=pltpu.VMEM)
    return pl.pallas_call(
        fused_kernel,
        out_shape=(
            jax.ShapeDtypeStruct((own // 2, width), bf16),
            jax.ShapeDtypeStruct((sink.shape[0], own), f32),
        ),
        in_specs=[hbm] * 10 + [pl.BlockSpec(memory_space=pltpu.SMEM), hbm] + [inside] * 3,
        out_specs=[inside] * 2,
        scratch_shapes=[
            vmem((2, 4, own, half_d), bf16),
            vmem((2, rows, half_d), bf16),
            vmem((2, rows, H), f32),
            vmem((2, 1, half_d), f32),
            vmem((rows, H), f32),
            vmem((2, 2, run_rows + 2 * edge, H), bf16),
            vmem((rows, 2 * H), bf16),
            vmem((3, rows, H), bf16),
            vmem((2, 2, 2, 2) + decay_log.shape, f32),
            vmem((2, 8, run_rows), f32),
            vmem((2, run_rows, H), f32),
            vmem((2, 2, 8, H), f32),
            vmem((2, H, 2 * H), bf16),
            vmem((2, 2, 2, 2, H, H), bf16),
            vmem((2, 4 * edge, 3 * H), bf16),
            vmem((2 * edge, H), f32),
            vmem((4, 2, 2 * edge), f32),
            vmem((4, 2, 2 * edge), f32),
            vmem(tile, f32), vmem(tile, bf16), vmem(tile, bf16),
            vmem((8, 2, 2, edge, own), bf16), vmem((8, 2, 2, edge, own), bf16),
            vmem((8, 2, edge, own), bf16), vmem((8, 2, edge, own), bf16),
            dma((3,)), dma((2,)), dma((1,)), dma((4,)), dma((2, 4)), dma((2,)), dma((2, 4)),
            dma((2, 4)), dma((2, 3)), dma((2, 3)),
            dma((8,)), dma((8,)), dma((8, 2)), dma((8, 2)), dma((8, 2)), dma((8, 2)),
        ]
        + stream((depth, 4 * H))
        + stream((depth, 3 * H))
        + stream((out_rows, own)),
        compiler_params=pltpu.CompilerParams(
            collective_id=0, has_side_effects=True, vmem_limit_bytes=67043328
        ),
        cost_estimate=pl.CostEstimate(
            flops=10**11, bytes_accessed=2 * 10**7, transcendentals=0
        ),
    )(
        tokens, gain.reshape(1, half_d), *args[2:10], sink, decay_log, cos_t, sin_t, base
    )


def attend(query, key, value, sink, offset, total_rows):
    rows, kv, group, _ = query.shape
    ext = halo(jnp.stack([key, value]), "t", SPAN_RADIUS)
    size = min(rows, BLOCK)
    count = rows // size
    span = size + 2 * SPAN_RADIUS
    pieces = jnp.stack([ext[:, b * size : b * size + span] for b in range(count)])
    blocks = query.reshape(count, size, kv, group, HEAD_DIM)
    scores = jnp.einsum(
        "bqhgd,bkhd->bhgqk", blocks, pieces[:, 0], preferred_element_type=jnp.float32
    ) * HEAD_DIM ** (-0.5)
    base = offset + jnp.arange(count, dtype=jnp.int32) * size
    query_pos = base[:, None] + jnp.arange(size, dtype=jnp.int32)
    key_pos = base[:, None] - SPAN_RADIUS + jnp.arange(span, dtype=jnp.int32)
    spacing = key_pos[:, None, :] - query_pos[:, :, None]
    inside = (key_pos >= 0) & (key_pos < total_rows)
    valid = (jnp.abs(spacing) <= SPAN_RADIUS) & inside[:, None, :]
    masked = jnp.where(valid[:, None, None], scores, -jnp.inf)
    limit = sink[None, :, :, None]
    top = jnp.maximum(jnp.max(masked, axis=-1), limit)
    expo = jnp.exp(masked - top[..., None])
    total = jnp.sum(expo, axis=-1) + jnp.exp(limit - top)
    logs = top + jnp.log(total)
    probs = (expo / total[..., None]).astype(jnp.bfloat16)
    result = jnp.einsum(
        "bhgqk,bkhd->bqhgd", probs, pieces[:, 1], preferred_element_type=jnp.float32
    ).astype(jnp.bfloat16)
    logs = jnp.transpose(logs, (1, 2, 0, 3)).reshape(kv * group, rows)
    return result.reshape(rows, kv * group * HEAD_DIM), logs


def retain(query, key, value, decay):
    rows, heads, _ = query.shape
    peers, index = lax.axis_size("t"), lax.axis_index("t")
    cumul = jnp.cumsum(decay, axis=1)
    last = cumul[:, -1]
    query_f, key_f, value_f = (v.astype(jnp.float32) for v in (query, key, value))
    trailing = jnp.exp(last[:, None] - cumul)
    leading = jnp.exp(cumul)
    forward = jnp.einsum("hk,khd,khe->hde", trailing, key_f, value_f, precision=HIGHEST)
    backward = jnp.einsum("hk,khd,khe->hde", leading, key_f, value_f, precision=HIGHEST)
    tail = jnp.broadcast_to(last[:, None, None], (heads, 8, HEAD_DIM))
    sent = jnp.concatenate([forward, backward, tail], axis=1)
    seen = lax.all_gather(sent, "t", axis=0)
    lasts = seen[:, :, 2 * HEAD_DIM, 0]
    at = jnp.arange(peers)
    low = jnp.minimum(at, index)[:, None]
    high = jnp.maximum(at, index)[:, None]
    between = (at[None, :] > low) & (at[None, :] < high)
    spans = jnp.exp(jnp.sum(jnp.where(between[:, :, None], lasts[None], 0.0), axis=1))
    before = jnp.sum(
        jnp.where(at < index, 1.0, 0.0)[:, None, None, None]
        * spans[:, :, None, None]
        * seen[:, :, :HEAD_DIM],
        axis=0,
    )
    after = jnp.sum(
        jnp.where(at > index, 1.0, 0.0)[:, None, None, None]
        * spans[:, :, None, None]
        * seen[:, :, HEAD_DIM : 2 * HEAD_DIM],
        axis=0,
    )
    scores = jnp.einsum("qhd,khd->hqk", query, key, preferred_element_type=jnp.float32)
    weights = jnp.exp(-jnp.abs(cumul[:, :, None] - cumul[:, None, :]))
    mix = jnp.einsum("hqk,khd->qhd", scores * weights, value_f, precision=HIGHEST)
    mix = mix + leading.T[:, :, None] * jnp.einsum(
        "qhd,hde->qhe", query_f, before, precision=HIGHEST
    )
    mix = mix + trailing.T[:, :, None] * jnp.einsum(
        "qhd,hde->qhe", query_f, after, precision=HIGHEST
    )
    middle = mix - jnp.mean(mix, axis=-1, keepdims=True)
    normed = middle * lax.rsqrt(jnp.mean(middle * middle, axis=-1, keepdims=True) + 1e-06)
    return normed.astype(jnp.bfloat16).reshape(rows, heads * HEAD_DIM)


def shards(
    tokens, gain, q_att, k_att, v_att, q_ret, k_ret, v_ret, out_att, out_ret, sink, decay_log
):
    parts = lax.axis_size("h")
    own = tokens.shape[0]
    rows = own * parts
    width = tokens.shape[1] * lax.axis_size("tp")
    kv = k_att.shape[1] // HEAD_DIM // parts
    group = q_att.shape[1] // k_att.shape[1]
    att = kv * group
    ret = q_ret.shape[1] // HEAD_DIM // parts
    offset = lax.axis_index("t") * rows
    total_rows = rows * lax.axis_size("t")

    packed = jnp.concatenate(
        [
            w.reshape(w.shape[0], parts, w.shape[1] // parts)
            for w in (q_att, k_att, v_att, q_ret, k_ret, v_ret)
        ],
        axis=2,
    )
    packed = jnp.moveaxis(packed, 1, 0)
    out_pack = jnp.concatenate(
        [w.reshape(parts, w.shape[0] // parts, w.shape[1]) for w in (out_att, out_ret)], axis=1
    )
    widened = tokens.astype(jnp.float32)
    sums = jnp.sum(widened * widened, axis=1)
    scaled = (widened * gain).astype(jnp.bfloat16)
    cores = lax.axis_size("tp")
    flat = packed.reshape(parts * packed.shape[1], packed.shape[2])
    weight = gather(exchange(flat, "h", 0, 0), "t", 0)
    whole = gather(gather(scaled, "h", 0), "tp", 1)
    proj = jnp.dot(whole, weight, preferred_element_type=jnp.float32)
    out_own = exchange(out_pack, "h", 0, 0)
    sums = lax.all_gather(sums, ("h", "tp"))
    decay = exchange(decay_log, "h", 0, 1)
    squares = jnp.sum(sums.reshape(parts, cores, own), axis=1).reshape(rows)
    inverse = lax.rsqrt(squares / width + 1e-06)[:, None]

    edges = [att, kv, kv, ret, ret, ret]
    starts = [sum(edges[:i]) * HEAD_DIM for i in range(6)]
    qa, ka, va, qr, kr, vr = (
        proj[:, s : s + n * HEAD_DIM].reshape(rows, n, HEAD_DIM) for s, n in zip(starts, edges)
    )
    scale = inverse[:, :, None]
    positions = (offset + jnp.arange(rows, dtype=jnp.int32)).astype(jnp.float32)
    freqs = 10000.0 ** (-jnp.arange(0, HEAD_DIM, 2).astype(jnp.float32) / HEAD_DIM)
    angles = positions[:, None] * freqs[None, :]
    cosine, sine = jnp.cos(angles)[:, None, :], jnp.sin(angles)[:, None, :]
    att_query = rotate(qa * scale, cosine, sine)
    att_key = rotate(ka * scale, cosine, sine)
    att_value = (va * scale).astype(jnp.bfloat16)
    ret_query = (qr * scale).astype(jnp.bfloat16)
    ret_key = (kr * (scale * HEAD_DIM ** (-0.5))).astype(jnp.bfloat16)
    ret_value = (vr * scale).astype(jnp.bfloat16)

    logits = lax.dynamic_slice_in_dim(sink, lax.axis_index("h") * att, att).reshape(kv, group)
    att_out, logs = attend(
        att_query.reshape(rows, kv, group, HEAD_DIM), att_key, att_value, logits, offset, total_rows
    )
    ret_out = retain(ret_query, ret_key, ret_value, decay)

    out_wide = gather(out_own, "t", 0)
    mixers = jnp.concatenate([att_out, ret_out], axis=1)
    depth = out_wide.shape[1]
    out_wide = jnp.moveaxis(out_wide, 0, 1).reshape(depth, -1)
    mixed = jnp.dot(mixers, out_wide, preferred_element_type=jnp.float32).astype(jnp.bfloat16)
    mixed = lax.psum_scatter(mixed, ("h", "tp"), scatter_dimension=0, tiled=True)
    return mixed, exchange(logs, "h", 1, 0)


def fits(args, sp, tp):
    tokens, _, q_att, k_att, v_att, q_ret, k_ret, v_ret, out_att, _, _, decay = args
    own, heads = tokens.shape[0] // sp, 4 * tp
    return (
        sp == 16
        and tp == 2
        and own == 2 * SPAN_RADIUS
        and q_att.shape[0] == sp * own
        and tokens.shape[1] == sp * own
        and q_att.shape[1] == 2 * heads * HEAD_DIM
        and all(v.shape[1] == heads * HEAD_DIM for v in (k_att, v_att, q_ret, k_ret, v_ret))
    )


def solution(mesh):
    sp, tp = mesh.shape["sp"], mesh.shape["tp"]

    def run(*args):
        if fits(args, sp, tp):
            seq = ("zh", "zl", "y", "x")
            fine = Mesh(mesh.devices.reshape(2, 2, 2, 2, tp), seq + ("tp",))
            step = fused
        else:
            heads = math.gcd(args[3].shape[1], args[5].shape[1]) // HEAD_DIM
            parts = math.gcd(heads // math.gcd(heads, tp), sp)
            seq = ("t", "h")
            fine = Mesh(mesh.devices.reshape(sp // parts, parts, tp), seq + ("tp",))
            step = shards
        body = jax.shard_map(
            step,
            mesh=fine,
            in_specs=(P(seq, "tp"), P("tp"))
            + (P(seq, "tp"),) * 6
            + (P("tp", seq), P("tp", seq), P("tp"), P("tp", seq)),
            out_specs=(P(seq + ("tp",), None), P("tp", seq)),
            check_vma=False,
        )
        return body(*args)

    return run
```

time: 310 us -> 238 us (0.77)
  Pallas kernels: 196 us -> 234 us
  blocking collectives: 26 us -> 0 us
  waiting for transfers between devices: 22.8 us -> 0 us
  local copies, waits for them, and re-layouts: 22 us -> 2.9 us
  other arithmetic: 15.5 us -> 0 us
  between operations: 15.8 us -> 0.65 us
  matrix products: 8.1 us -> 0 us
    pallas_call x2 -> x1, Pallas kernels: 196 us -> 234 us  [fused(): pl.pallas_call(fused_kernel, out_shape=(jax.ShapeDtypeStruct((own // 2, w...]
    all_gather x1 -> x0, blocking collectives: 26 us -> none  [retain(): seen = lax.all_gather(sent, 't', axis=0)]
    all_gather x1 -> x0, waiting for transfers between devices: 22.8 us -> none  [gather(): return lax.all_gather(x, axis, axis=dim, tiled=True)]
    dot_general x8 -> x0, matrix products: 8.1 us -> none  [the longest x1 2.76 us: retain(): jnp.einsum('hqk,khd->qhd', scores * weights, value_f, precision=HIGHEST)]
    unnamed x38 -> x4, local copies, waits for them, and re-layouts: 9.29 us -> 2.9 us
    reshape x10 -> x0, local copies, waits for them, and re-layouts: 5.8 us -> none  [the longest x1 1.55 us: shards(): proj[:, s:s + n * HEAD_DIM].reshape(rows, n, HEAD_DIM)]
    concatenate x4 -> x0, other arithmetic: 4.47 us -> none  [the longest x1 2.42 us: rotate(): jnp.concatenate([first * cosine - second * sine, second * cosine + first...]
    reduce_sum x6 -> x0, other arithmetic: 4.04 us -> none  [the longest x1 1.7 us: shards(): sums = jnp.sum(widened * widened, axis=1)]
  transfers between devices with their start and end apart: 3 -> 0, of which waited for: 1 -> 0; matrix products, arithmetic and copies ran while one was open for 8% -> 0% of each run, Pallas kernels for 0% -> 0%
where the time goes in v1:
time: 238 us
  Pallas kernels  234 us (98%)
  local copies, waits for them, and re-layouts  2.9 us (1%)
    pallas_call x1, Pallas kernels, fused(): pl.pallas_call(fused_kernel, out_shape=(jax.ShapeDtypeStruct((own // 2, w...  234 us

profile of v1, /device:TPU:0, one launch (start us, length us, event | category | flops | bytes accessed | tf_op | source)
XLA Modules:
  0.0 237.5 jit_solution(16163355192524069853)
XLA Ops:
  0.6 234.0 %shard_map.158 = (bf16[128,4096]{1,0:T(8,128)(2,1)}, f32[8,256]{1,0:T(8,128)}) custom-call(bf16[256,2048]{1,0:T(8,128)(2,1)} %tokens.1, f32[1,2048]{1,0:T(1,128)} %bitcast.1, bf16[256,1024]{1,0:T(8,128)(2,1)} %q_att.1, bf16[256,512]{1,0:T(8,128)(2,1)} %k_att.1, bf16[256,512]{1,0:T(8,128)(2,1)} %v_att.1, bf16[256,512]{1,0:T(8,128)(2,1)} %q_ret.1, ...), custom_call_target="tpu_custom_call" | custom-call | flops 99999997952 | bytes 20000000 | tf_op jit(solution)/shard_map/pallas_call | solution.py:820
  234.6 0.0 copy-start
  234.6 2.3 copy.19
  236.9 0.0 copy-done
  236.9 0.6 copy.20
Async XLA Ops:
  234.6 2.3 copy-start

commit v2 on v1

--- a/solution.py
+++ b/solution.py
@@ -243,36 +243,44 @@
 
     gain_c = remote(gains.at[w.c], gains.at[w.c], g_sem.at[0], g_sem.at[1], w.to_c)
 
-    d_parts = (
-        (dec.at[w.zh, w.y, w.zl, w.x], dec.at[w.zh, w.y, w.zl, 1 - w.x], w.to_x),
-        (dec.at[w.zh, w.y, w.zl], dec.at[w.zh, w.y, 1 - w.zl], w.to_z),
-        (dec.at[w.zh, w.y], dec.at[w.zh, 1 - w.y], w.to_y),
-        (dec.at[w.zh], dec.at[1 - w.zh], w.to_h),
-    )
-
-    def decay_send(k):
-        src, _, to = d_parts[k]
-        return remote(src, src, d_sem.at[0, k], d_sem.at[1, k], to)
-
-    def decay_arrive(k):
-        _, dst, to = d_parts[k]
-        remote(dst, dst, d_sem.at[0, k], d_sem.at[1, k], to).wait_recv()
-
+    def flip(v, bit):
+        return v + bit - 2 * v * bit
+
+    def others(i):
+        return tuple(flip(v, (i >> k) & 1) for v, k in ((w.zh, 3), (w.zl, 2), (w.y, 1), (w.x, 0)))
+
+    def decay_send(i):
+        zh, zl, y, x = others(i)
+        here = dec.at[w.zh, w.y, w.zl, w.x]
+        to = {"zh": zh, "zl": zl, "y": y, "x": x}
+        return remote(here, here, d_sem.at[0, i], d_sem.at[1, i], to)
+
+    def decay_arrive(i):
+        zh, zl, y, x = others(i)
+        here = dec.at[zh, y, zl, x]
+        to = {"zh": zh, "zl": zl, "y": y, "x": x}
+        remote(here, here, d_sem.at[0, i], d_sem.at[1, i], to).wait_recv()
+
+    decay_load.start()
     A.fetch()
+    gain_load.start()
     token_load.start()
-    gain_load.start()
-    decay_load.start()
     R.fetch()
     O.fetch()
 
     barrier = pltpu.get_barrier_semaphore()
-    friends = (w.to_x, w.to_z, w.to_y, w.to_h, w.to_hy, w.to_zx, w.to_c)
-    for to in friends:
+    pl.semaphore_signal(barrier, inc=1, device_id=w.to_c, device_id_type=MESH)
+    for i in range(1, 16):
+        zh, zl, y, x = others(i)
+        to = {"zh": zh, "zl": zl, "y": y, "x": x}
         pl.semaphore_signal(barrier, inc=1, device_id=to, device_id_type=MESH)
-    pl.semaphore_wait(barrier, len(friends))
+    pl.semaphore_wait(barrier, 16)
 
     middle = w.g == 1
 
+    decay_load.wait()
+    for i in range(1, 16):
+        decay_send(i).start()
     A.fetched()
     A.along_x(0).start()
     A.along_z(0).start()
@@ -289,10 +297,8 @@
         A.along_h(0).start()
         R.along_h(0).start()
 
-    decay_load.wait()
     gain_load.wait()
     gain_c.start()
-    decay_send(0).start()
     token_load.wait()
     tokens_x[0].start()
     tokens_c(0).start()
@@ -320,13 +326,9 @@
     scale(w.c, w.b)
     A.arrive_away()
     A.along_z(1).start()
-    decay_arrive(0)
-    decay_send(1).start()
     R.arrive_away()
     R.along_z(1).start()
     tokens_z.start()
-    decay_arrive(1)
-    decay_send(2).start()
     remote(gains.at[1 - w.c], gains.at[1 - w.c], g_sem.at[0], g_sem.at[1], w.to_c).wait_recv()
     token_arrive(0, 1 - w.c)
     scale(1 - w.c, w.b)
@@ -346,9 +348,8 @@
         for k in range(4):
             R.along_h(k).start()
 
-    decay_arrive(2)
-    decay_send(3).start()
-    decay_arrive(3)
+    for i in range(1, 16):
+        decay_arrive(i)
 
     lane = lax.broadcasted_iota(jnp.int32, (8, run_rows), 1)
     for slot in range(2):
@@ -770,7 +771,8 @@
         stream.drain()
     for k in range(4):
         tokens_c(k).wait_send()
-        decay_send(k).wait_send()
+    for i in range(1, 16):
+        decay_send(i).wait_send()
     for copy in tokens_x + (tokens_z, gain_c):
         copy.wait_send()
     for copy in halo_y + state_sends + log_sends:
@@ -847,7 +849,7 @@
             vmem(tile, f32), vmem(tile, bf16), vmem(tile, bf16),
             vmem((8, 2, 2, edge, own), bf16), vmem((8, 2, 2, edge, own), bf16),
             vmem((8, 2, edge, own), bf16), vmem((8, 2, edge, own), bf16),
-            dma((3,)), dma((2,)), dma((1,)), dma((4,)), dma((2, 4)), dma((2,)), dma((2, 4)),
+            dma((3,)), dma((2,)), dma((1,)), dma((4,)), dma((2, 4)), dma((2,)), dma((2, 16)),
             dma((2, 4)), dma((2, 3)), dma((2, 3)),
             dma((8,)), dma((8,)), dma((8, 2)), dma((8, 2)), dma((8, 2)), dma((8, 2)),
         ]

time: 238 us -> 189 us (0.79)
  Pallas kernels: 234 us -> 185 us
    pallas_call x1, Pallas kernels: 234 us -> 185 us  [fused(): pl.pallas_call(fused_kernel, out_shape=(jax.ShapeDtypeStruct((own // 2, w...]
where the time goes in v2:
time: 189 us; the launch traced here: 188 us
  Pallas kernels  185 us (98%)
  local copies, waits for them, and re-layouts  2.9 us (2%)
    pallas_call x1, Pallas kernels, fused(): pl.pallas_call(fused_kernel, out_shape=(jax.ShapeDtypeStruct((own // 2, w...  185 us

profile of v2, /device:TPU:0, one launch (start us, length us, event | category | flops | bytes accessed | tf_op | source)
XLA Modules:
  0.0 188.4 jit_solution(6982758804080833217)
XLA Ops:
  0.6 184.8 %shard_map.158 = (bf16[128,4096]{1,0:T(8,128)(2,1)}, f32[8,256]{1,0:T(8,128)}) custom-call(bf16[256,2048]{1,0:T(8,128)(2,1)} %tokens.1, f32[1,2048]{1,0:T(1,128)} %bitcast.1, bf16[256,1024]{1,0:T(8,128)(2,1)} %q_att.1, bf16[256,512]{1,0:T(8,128)(2,1)} %k_att.1, bf16[256,512]{1,0:T(8,128)(2,1)} %v_att.1, bf16[256,512]{1,0:T(8,128)(2,1)} %q_ret.1, ...), custom_call_target="tpu_custom_call" | custom-call | flops 99999997952 | bytes 20000000 | tf_op jit(solution)/shard_map/pallas_call | solution.py:822
  185.5 0.0 copy-start
  185.5 2.3 %copy.19 = bf16[128,4096]{1,0:T(8,128)(2,1)} copy(bf16[128,4096]{1,0:T(8,128)(2,1)} %get-tuple-element.4) | data formatting | bytes 2097152
  187.8 0.0 copy-done
  187.8 0.6 copy.20
Async XLA Ops:
  185.5 2.3 %copy-start = (f32[8,256]{1,0:T(8,128)S(1)}, f32[8,256]{1,0:T(8,128)}, u32[]{:S(2)}) copy-start(f32[8,256]{1,0:T(8,128)} %get-tuple-element.5) | copy-start | bytes 24580

commit v3 on v2

--- a/solution.py
+++ b/solution.py
@@ -45,6 +45,10 @@
     ).astype(jnp.bfloat16)
 
 
+def flip(v, bit):
+    return v + bit - 2 * v * bit
+
+
 class Stream:
     def __init__(self, where, remote, refs, pack):
         self.where, self.remote, self.pack = where, remote, pack
@@ -92,11 +96,15 @@
 
     def near(self, k):
         w = self.where
-        return w.at(w.zh, (w.zl, 1 - w.zl)[k // 2], w.y, (w.x, 1 - w.x)[k % 2])
+        return w.at(w.zh, flip(w.zl, k // 2), w.y, flip(w.x, k % 2))
 
     def far(self, k):
         w = self.where
-        return w.at(1 - w.zh, (w.zl, 1 - w.zl)[1 - k // 2], w.y, (w.x, 1 - w.x)[k % 2])
+        return w.at(1 - w.zh, flip(w.zl, 1 - k // 2), w.y, flip(w.x, k % 2))
+
+    def across(self, k):
+        w = self.where
+        return w.at(1 - w.zh, flip(w.zl, 1 - k // 2), 1 - w.y, flip(w.x, k % 2))
 
     def along_h(self, k):
         s = self.near(k)
@@ -104,10 +112,11 @@
             self.wide.at[s], self.wide.at[s], self.h_send.at[k], self.w_recv.at[s], self.where.to_h
         )
 
-    def along_y(self, k):
-        s = self.near(k) if k < 4 else self.far(k - 4)
+    def along_y(self, k, far=0):
+        s = self.far(k) if far else self.near(k)
         return self.remote(
-            self.wide.at[s], self.wide.at[s], self.y_send.at[k], self.w_recv.at[s], self.where.to_y
+            self.wide.at[s], self.wide.at[s],
+            self.y_send.at[4 * far + k], self.w_recv.at[s], self.where.to_y,
         )
 
     def arrive(self, s):
@@ -120,12 +129,12 @@
         slot = self.away.at[1 - w.x]
         self.remote(slot, slot, self.x_send.at[0], self.p_recv.at[0], w.to_x).wait_recv()
 
-    def arrive_across(self):
+    def arrive_across(self, far):
         w = self.where
-        for zh in (w.zh, 1 - w.zh):
-            for zl in range(2):
-                for x in range(2):
-                    self.arrive(w.at(zh, zl, 1 - w.y, x))
+        zh = 1 - w.zh if far else w.zh
+        for zl in range(2):
+            for x in range(2):
+                self.arrive(w.at(zh, zl, 1 - w.y, x))
 
     def drain(self):
         for k in range(2):
@@ -133,8 +142,8 @@
             self.along_z(k).wait_send()
         for k in range(4):
             self.along_h(k).wait_send()
-        for k in range(8):
             self.along_y(k).wait_send()
+            self.along_y(k, 1).wait_send()
 
 
 class Place:
@@ -153,6 +162,7 @@
         self.to_hy = {"zh": 1 - self.zh, "zl": 1 - self.zl, "y": 1 - self.y}
         self.to_zx = {"zl": 1 - self.zl, "x": 1 - self.x}
         self.to_c = {"tp": 1 - self.c}
+        self.to_zc = {"zl": 1 - self.zl, "tp": 1 - self.c}
 
     @staticmethod
     def at(zh, zl, y, x):
@@ -163,13 +173,14 @@
     tokens, gain, q_att, k_att, v_att, q_ret, k_ret, v_ret, out_att, out_ret, sink, decay,
     cos_t, sin_t, base,
     mixed, logs_out,
-    raw, scl, ssq, gains, proj, kvext, qrot, rets, dec, cumr, cumc, coef, states, stall,
+    raw, scl, ssq, gains, acc_a, acc_r, kvext, qrot, rets, dec, cumr, cumc, coef, states, stall, crossing,
     mix, logm, lsend, lrecv, mine, give, take, s1, r1, s2, r2,
-    t_load, t_x, t_z, t_c, t_recv, g_sem, d_sem, halo_sem, st_sem, l_sem,
+    t_load, t_x, t_z, t_c, t_recv, g_sem, d_sem, halo_sem, st_sem, l_sem, go,
     give_s, take_r, s1_s, r1_r, s2_s, r2_r,
     *streams,
 ):
     w = Place()
+    y = w.y
     f32, bf16 = jnp.float32, jnp.bfloat16
     own, half_d = tokens.shape
     rows = 4 * own
@@ -221,90 +232,87 @@
     def block(zl, x):
         return 2 * zl + x
 
-    def token(b, send, to):
-        here = raw.at[w.c, b]
-        return remote(here, here, send, t_recv.at[w.c, b], to)
-
-    tokens_x = (
-        token(w.b, t_x.at[0], w.to_x),
-        token(block(1 - w.zl, w.x), t_x.at[1], w.to_x),
-    )
-    tokens_z = token(w.b, t_z.at[0], w.to_z)
-
-    def tokens_c(k):
-        b = block((w.zl, 1 - w.zl)[k // 2], (w.x, 1 - w.x)[k % 2])
-        return token(b, t_c.at[k], w.to_c)
-
-    def token_arrive(k, e=None):
-        b = block((w.zl, 1 - w.zl)[k // 2], (w.x, 1 - w.x)[k % 2])
-        e = w.c if e is None else e
-        here = raw.at[e, b]
-        remote(here, here, t_x.at[0], t_recv.at[e, b], w.to_x).wait_recv()
+    def order(k):
+        return block((w.zl, 1 - w.zl)[k // 2], (w.x, 1 - w.x)[k % 2])
+
+    def token(e, k, part, send, to):
+        here = raw.at[e, order(k)]
+        if part is not None:
+            here = here.at[pl.ds(part * edge, edge), :]
+        return remote(here, here, send, t_recv.at[e, order(k), part or 0], to)
+
+    tokens_x = [token(w.c, 0, None, t_x.at[0], w.to_x)]
+    tokens_x += [token(w.c, 2, i, t_x.at[1 + i], w.to_x) for i in range(2)]
+    tokens_z = token(w.c, 0, None, t_z.at[0], w.to_z)
+    tokens_c = [token(w.c, k, None, t_c.at[k], w.to_c) for k in range(3)]
+    tokens_c += [token(w.c, 3, i, t_c.at[3 + i], w.to_c) for i in range(2)]
+
+    def token_arrive(k, e=None, part=None):
+        token(w.c if e is None else e, k, part, t_x.at[0], w.to_x).wait_recv()
 
     gain_c = remote(gains.at[w.c], gains.at[w.c], g_sem.at[0], g_sem.at[1], w.to_c)
-
-    def flip(v, bit):
-        return v + bit - 2 * v * bit
 
     def others(i):
         return tuple(flip(v, (i >> k) & 1) for v, k in ((w.zh, 3), (w.zl, 2), (w.y, 1), (w.x, 0)))
 
+    def peer(i):
+        return dict(zip(("zh", "zl", "y", "x"), others(i)))
+
     def decay_send(i):
-        zh, zl, y, x = others(i)
         here = dec.at[w.zh, w.y, w.zl, w.x]
-        to = {"zh": zh, "zl": zl, "y": y, "x": x}
-        return remote(here, here, d_sem.at[0, i], d_sem.at[1, i], to)
+        return remote(here, here, d_sem.at[0, i], d_sem.at[1, i], peer(i))
 
     def decay_arrive(i):
-        zh, zl, y, x = others(i)
-        here = dec.at[zh, y, zl, x]
-        to = {"zh": zh, "zl": zl, "y": y, "x": x}
-        remote(here, here, d_sem.at[0, i], d_sem.at[1, i], to).wait_recv()
+        zh, zl, yy, x = others(i)
+        here = dec.at[zh, yy, zl, x]
+        remote(here, here, d_sem.at[0, i], d_sem.at[1, i], peer(i)).wait_recv()
 
     decay_load.start()
+    R.fetch()
     A.fetch()
     gain_load.start()
     token_load.start()
-    R.fetch()
     O.fetch()
 
     barrier = pltpu.get_barrier_semaphore()
-    pl.semaphore_signal(barrier, inc=1, device_id=w.to_c, device_id_type=MESH)
+    for to in (w.to_c, w.to_zc):
+        pl.semaphore_signal(barrier, inc=1, device_id=to, device_id_type=MESH)
     for i in range(1, 16):
-        zh, zl, y, x = others(i)
-        to = {"zh": zh, "zl": zl, "y": y, "x": x}
-        pl.semaphore_signal(barrier, inc=1, device_id=to, device_id_type=MESH)
-    pl.semaphore_wait(barrier, 16)
+        pl.semaphore_signal(barrier, inc=1, device_id=peer(i), device_id_type=MESH)
+    pl.semaphore_wait(barrier, 17)
 
     middle = w.g == 1
 
     decay_load.wait()
     for i in range(1, 16):
         decay_send(i).start()
+    R.fetched()
+    R.along_x(0).start()
+    R.along_z(0).start()
+    R.along_y(0).start()
     A.fetched()
     A.along_x(0).start()
     A.along_z(0).start()
     A.along_y(0).start()
-    R.fetched()
-    R.along_x(0).start()
-    R.along_z(0).start()
-    R.along_y(0).start()
+    R.along_x(1).start()
     A.along_x(1).start()
-    R.along_x(1).start()
 
     @pl.when(middle)
     def _():
+        R.along_h(0).start()
         A.along_h(0).start()
-        R.along_h(0).start()
-
+
+    O.fetched()
+    O.along_x(1).start()
+    O.along_x(0).start()
+    token_load.wait()
+    tokens_x[0].start()
     gain_load.wait()
     gain_c.start()
-    token_load.wait()
-    tokens_x[0].start()
-    tokens_c(0).start()
-
-    def scale(e, b):
-        @pl.loop(0, own // 16)
+    tokens_c[0].start()
+
+    def scale(e, b, first=0, last=None):
+        @pl.loop(first // 16, (own if last is None else last) // 16)
         def _(i):
             value = raw[e, b, pl.ds(pl.multiple_of(i * 16, 16), 16), :].astype(f32)
             at = pl.ds(pl.multiple_of(b * own + i * 16, 16), 16)
@@ -324,29 +332,44 @@
         kvext[1, :, edge + run_rows :, :] = jnp.zeros((2, edge, H), bf16)
 
     scale(w.c, w.b)
-    A.arrive_away()
-    A.along_z(1).start()
-    R.arrive_away()
-    R.along_z(1).start()
+    for stream in (R, A):
+        stream.arrive_away()
+        stream.along_z(1).start()
     tokens_z.start()
     remote(gains.at[1 - w.c], gains.at[1 - w.c], g_sem.at[0], g_sem.at[1], w.to_c).wait_recv()
     token_arrive(0, 1 - w.c)
     scale(1 - w.c, w.b)
-    for k in (2, 1, 3):
-        for stream in (A, R):
-            stream.arrive(stream.near(k))
-            stream.along_y(k).start()
-
-            @pl.when(middle)
-            def _():
+
+    def pass_near(stream, k):
+        stream.arrive(stream.near(k))
+        stream.along_y(k).start()
+
+        @pl.when(middle)
+        def _():
+            stream.along_h(k).start()
+
+    def pass_far(stream, k):
+        stream.arrive(stream.far(k))
+        stream.along_y(k, 1).start()
+
+    pass_near(R, 2)
+    pass_near(A, 2)
+    for k in (1, 3):
+        pass_near(R, k)
+        pass_near(A, k)
+
+    O.along_y(0).start()
+    O.along_z(0).start()
+
+    @pl.when(w.g == 0)
+    def _():
+        for stream in (R, A):
+            for k in range(4):
                 stream.along_h(k).start()
 
-    @pl.when(w.g == 0)
-    def _():
-        for k in range(4):
-            A.along_h(k).start()
-        for k in range(4):
-            R.along_h(k).start()
+    @pl.when(middle)
+    def _():
+        O.along_h(0).start()
 
     for i in range(1, 16):
         decay_arrive(i)
@@ -368,62 +391,129 @@
     totals = jnp.zeros((8, H), f32)
     for zh in range(2):
         for slot in range(2):
-            for y in range(2):
-                pair = sum(dec[zh, y, slot, x, pl.ds(w.h, 1), :] for x in range(2))
+            for yy in range(2):
+                pair = sum(dec[zh, yy, slot, x, pl.ds(w.h, 1), :] for x in range(2))
                 value = jnp.sum(pair, axis=1, keepdims=True)
-                totals = jnp.where(lane == 4 * zh + 2 * slot + y, value, totals)
+                totals = jnp.where(lane == 4 * zh + 2 * slot + yy, value, totals)
     for slot in range(2):
         me = 4 * w.zh + 2 * slot + w.y
         between = (lane > jnp.minimum(run, me)) & (lane < jnp.maximum(run, me))
         factor = jnp.exp(jnp.sum(jnp.where(between, totals, 0.0), axis=1, keepdims=True))
         factor = jnp.broadcast_to(factor, (8, H))
-        coef[slot, 0] = jnp.where(run < me, factor, 0.0)
-        coef[slot, 1] = jnp.where(run > me, factor, 0.0)
-
-    token_arrive(2)
-    tokens_x[1].start()
-    tokens_c(2).start()
-    token_arrive(1)
-    tokens_c(1).start()
-    O.fetched()
-    O.along_x(0).start()
-    O.along_x(1).start()
-    for k in (2, 1):
-        b = block((w.zl, 1 - w.zl)[k // 2], (w.x, 1 - w.x)[k % 2])
-        scale(w.c, b)
-    for k in (2, 1):
-        b = block((w.zl, 1 - w.zl)[k // 2], (w.x, 1 - w.x)[k % 2])
-        token_arrive(k, 1 - w.c)
-        scale(1 - w.c, b)
-    for k in range(4):
-        A.arrive(A.far(k))
-        A.along_y(4 + k).start()
-
-    def pass_far(stream, k):
-        stream.arrive(stream.far(k))
-        stream.along_y(4 + k).start()
+        near = run // 4 == w.zh
+        coef[slot, 0] = jnp.where(near & (run < me), factor, 0.0)
+        coef[slot, 1] = jnp.where(near & (run > me), factor, 0.0)
+        between = (lane > jnp.where(w.zh == 0, me, 3)) & (lane < jnp.where(w.zh == 0, 4, me))
+        factor = jnp.exp(jnp.sum(jnp.where(between, totals, 0.0), axis=1, keepdims=True))
+        coef[slot, 2] = jnp.broadcast_to(factor, (8, H))
 
     @pl.when(middle)
     def _():
-        for k in range(4):
-            pass_far(R, k)
-
-    token_arrive(3)
-    tokens_c(3).start()
-    b3 = block(1 - w.zl, 1 - w.x)
-    scale(w.c, b3)
-    token_arrive(3, 1 - w.c)
-    scale(1 - w.c, b3)
-    O.along_z(0).start()
-    A.arrive_across()
-
-    def project(stream, b, start, width):
+        pass_near(O, 1)
+        for stream in (R, A):
+            for k in (0, 2, 1, 3):
+                pass_far(stream, k)
+
+    def part_of(stream, zh, b, start, width):
         at = pl.ds(pl.multiple_of(b * own, own), own)
         depth = half_d // own
-        first = stream.wide[0:depth, :, start : start + width].reshape(half_d, width)
-        second = stream.wide[depth : 2 * depth, :, start : start + width].reshape(half_d, width)
-        value = jnp.dot(scl[0, at, :], first, preferred_element_type=f32)
-        return value + jnp.dot(scl[1, at, :], second, preferred_element_type=f32)
+        weight = stream.wide[pl.ds(zh * depth, depth), :, start : start + width]
+        return jnp.dot(
+            scl[zh, at, :], weight.reshape(half_d, width), preferred_element_type=f32
+        )
+
+    def first_part(stream, acc, b):
+        at = pl.ds(pl.multiple_of(b * own, own), own)
+        start = 0
+        while start < acc.shape[1]:
+            width = min(2 * H, acc.shape[1] - start)
+            acc[at, start : start + width] = part_of(stream, w.zh, b, start, width)
+            start += width
+
+    def pair_of(stream, zl, yy, b, start, width):
+        zh = 1 - w.zh
+        at = pl.ds(pl.multiple_of(b * own, own), own)
+        depth = pl.ds(pl.multiple_of((2 * zl + yy) * 2 * own, 2 * own), 2 * own)
+        weight = stream.wide[pl.ds(w.at(zh, zl, yy, 0), 2), :, start : start + width]
+        return jnp.dot(
+            scl[zh, at, depth], weight.reshape(2 * own, width), preferred_element_type=f32
+        )
+
+    def add_pair(stream, acc, zl, yy, b):
+        at = pl.ds(pl.multiple_of(b * own, own), own)
+        for start in range(0, acc.shape[1], 2 * H):
+            width = min(2 * H, acc.shape[1] - start)
+            acc[at, start : start + width] += pair_of(stream, zl, yy, b, start, width)
+
+    def last_of(stream, acc, b, start, width):
+        at = pl.ds(pl.multiple_of(b * own, own), own)
+        return acc[at, start : start + width] + pair_of(stream, w.zl, 1 - w.y, b, start, width)
+
+    def whole_of(stream, acc, b, start, width):
+        at = pl.ds(pl.multiple_of(b * own, own), own)
+        return acc[at, start : start + width] + part_of(stream, 1 - w.zh, b, start, width)
+
+    token_arrive(2)
+    for copy in tokens_x[1:]:
+        copy.start()
+    tokens_c[2].start()
+    scale(w.c, order(2))
+    token_arrive(2, 1 - w.c)
+    scale(1 - w.c, order(2))
+    token_arrive(1)
+    tokens_c[1].start()
+    scale(w.c, order(1))
+
+    @pl.when(w.g == 0)
+    def _():
+        pass_far(R, 0)
+
+    O.arrive_away()
+    O.along_z(1).start()
+    token_arrive(1, 1 - w.c)
+    scale(1 - w.c, order(1))
+
+    @pl.when(w.g == 0)
+    def _():
+        pass_far(R, 1)
+
+    R.arrive_across(0)
+    A.arrive_across(0)
+
+    @pl.loop(0, 3)
+    def _(i):
+        k = 2 - i
+        b = block(flip(w.zl, k // 2), flip(w.x, k % 2))
+        first_part(R, acc_r, b)
+        first_part(A, acc_a, b)
+
+    @pl.when(w.g == 0)
+    def _():
+        pass_far(R, 2)
+
+    token_arrive(3, None, 0)
+    tokens_c[3].start()
+    scale(w.c, order(3), 0, edge)
+    token_arrive(3, 1 - w.c, 0)
+    scale(1 - w.c, order(3), 0, edge)
+
+    @pl.when(w.g == 0)
+    def _():
+        pass_far(R, 3)
+        pass_far(A, 0)
+
+    token_arrive(3, None, 1)
+    tokens_c[4].start()
+
+    @pl.when(w.g == 0)
+    def _():
+        pass_far(A, 1)
+
+    scale(w.c, order(3), edge, own)
+    token_arrive(3, 1 - w.c, 1)
+    scale(1 - w.c, order(3), edge, own)
+    first_part(R, acc_r, order(3))
+    first_part(A, acc_a, order(3))
 
     def inverse(b):
         at = pl.ds(pl.multiple_of(b * own, own), own)
@@ -440,23 +530,103 @@
     def turn(value, cosine, sine):
         return (value * cosine + pltpu.roll(value, H // 2, axis=1) * sine).astype(bf16)
 
-    def attention_inputs(b):
+    def keys_values(b):
+        scale_b = inverse(b)
+        cosine, sine = angles(b)
+        both = last_of(A, acc_a, b, 2 * H, 2 * H) * scale_b
+        inner = pl.ds(pl.multiple_of(edge + (b % 2) * own, edge), own)
+        kvext[b // 2, 0, inner, :] = turn(both[:, :H], cosine, sine)
+        kvext[b // 2, 1, inner, :] = both[:, H:].astype(bf16)
+
+    def queries(b):
+        at = pl.ds(pl.multiple_of(b * own, own), own)
+        cosine, sine = angles(b)
+        query = last_of(A, acc_a, b, 0, 2 * H) * inverse(b)
+        qrot[at, :H] = turn(query[:, :H], cosine, sine)
+        qrot[at, H:] = turn(query[:, H:], cosine, sine)
+
+    R.arrive_across(1)
+
+    def retention_inputs(b):
         at = pl.ds(pl.multiple_of(b * own, own), own)
         scale_b = inverse(b)
-        cosine, sine = angles(b)
-        query = project(A, b, 0, 2 * H) * scale_b
-        qrot[at, :H] = turn(query[:, :H], cosine, sine)
-        qrot[at, H:] = turn(query[:, H:], cosine, sine)
-        other = project(A, b, 2 * H, 2 * H) * scale_b
-        inner = pl.ds(pl.multiple_of(edge + (b % 2) * own, edge), own)
-        kvext[b // 2, 0, inner, :] = turn(other[:, :H], cosine, sine)
-        kvext[b // 2, 1, inner, :] = other[:, H:].astype(bf16)
+        both = whole_of(R, acc_r, b, 0, 2 * H)
+        rets[0, at, :] = (both[:, :H] * scale_b).astype(bf16)
+        rets[1, at, :] = (both[:, H:] * (scale_b * H ** (-0.5))).astype(bf16)
+        rets[2, at, :] = (whole_of(R, acc_r, b, 2 * H, H) * scale_b).astype(bf16)
+
+    @pl.when(w.g == 0)
+    def _():
+        pass_far(A, 2)
 
     @pl.loop(0, 4)
     def _(b):
-        attention_inputs(b)
-
-    y = w.y
+        retention_inputs(b)
+
+    for slot in range(2):
+        at = pl.ds(slot * run_rows, run_rows)
+        last = cumr[slot, 0:1, run_rows - 1 : run_rows]
+        key, value = rets[1, at, :].astype(f32), rets[2, at, :]
+        for i, weight in enumerate((jnp.exp(last - cumc[slot]), jnp.exp(cumc[slot]))):
+            lhs = (key * weight).astype(bf16)
+            state = lax.dot_general(
+                lhs, value, (((0,), (0,)), ((), ())), preferred_element_type=f32
+            ).astype(bf16)
+            stall[y, slot, i] = state
+    total = jnp.zeros((H, H), f32)
+    for slot in range(2):
+        total = total + coef[slot, 2, 0:1, :] * stall[y, slot, w.zh].astype(f32)
+    crossing[2] = total.astype(bf16)
+    state_sends = [
+        remote(stall.at[y], stall.at[y], st_sem.at[0, 0], st_sem.at[1, 0], w.to_y),
+        remote(crossing.at[2], crossing.at[0], st_sem.at[0, 1], st_sem.at[1, 1], w.to_h),
+        remote(crossing.at[2], crossing.at[1], st_sem.at[0, 2], st_sem.at[1, 2], w.to_hy),
+    ]
+    state_sends[1].start()
+    state_sends[2].start()
+
+    def inner_tile(i):
+        slot = i // 2
+        at = pl.ds(pl.multiple_of(i * own, own), own)
+        keys = pl.ds(pl.multiple_of(slot * run_rows, run_rows), run_rows)
+        score = lax.dot_general(
+            rets[0, at, :], rets[1, keys, :], (((1,), (1,)), ((), ())),
+            preferred_element_type=f32,
+        )
+        column = cumc[slot, pl.ds(pl.multiple_of((i % 2) * own, own), own), :]
+        column = jnp.concatenate([column] * (run_rows // H), axis=1)
+        weight = jnp.exp(-jnp.abs(column - cumr[slot, 0:1, :]))
+        acc_r[at, :H] = jnp.dot(
+            (score * weight).astype(bf16), rets[2, keys, :], preferred_element_type=f32
+        )
+
+    @pl.loop(0, 4)
+    def _(i):
+        inner_tile(i)
+
+    @pl.when(w.g == 0)
+    def _():
+        pass_far(A, 3)
+
+    @pl.loop(0, 8)
+    def _(i):
+        add_pair(A, acc_a, i // 4, y, i % 4)
+
+    for k in range(2):
+        A.arrive(A.across(k))
+
+    @pl.loop(0, 4)
+    def _(b):
+        add_pair(A, acc_a, 1 - w.zl, 1 - y, b)
+
+    state_sends[0].start()
+    for k in range(2, 4):
+        A.arrive(A.across(k))
+
+    @pl.loop(0, 4)
+    def _(b):
+        keys_values(b)
+
     head, tail, before_at, after_at = edge, run_rows, 0, edge + run_rows
 
     def pick(a, b):
@@ -490,27 +660,20 @@
     def _():
         halo_far.start()
 
-    @pl.when(w.g == 0)
-    def _():
-        for k in range(4):
-            pass_far(R, k)
-
-    O.along_y(0).start()
-    O.along_h(0).start()
-    O.arrive_away()
-    O.along_z(1).start()
+    @pl.when(middle)
+    def _():
+        for k in (2, 3):
+            pass_near(O, k)
+        for k in range(2):
+            pass_far(O, k)
+
+    @pl.loop(0, 4)
+    def _(b):
+        queries(b)
 
     def halo_arrive(slot, start, i, to):
         here = piece(slot, start)
         remote(here, here, halo_sem.at[0, i], halo_sem.at[1, i], to).wait_recv()
-
-    halo_arrive(pick(0, 0), pick(after_at, before_at), 0, w.to_y)
-    halo_arrive(pick(1, 0), pick(before_at, after_at), 1, w.to_y)
-    halo_arrive(pick(1, 1), pick(after_at, before_at), 2, w.to_y)
-
-    @pl.when(has_far)
-    def _():
-        halo_arrive(pick(0, 1), pick(before_at, after_at), 3, w.to_hy)
 
     def attend_tile(i):
         slot, j = i // 4, i % 4
@@ -547,19 +710,73 @@
 
     @pl.loop(0, 4)
     def _(i):
-        attend_tile(i)
-
-    for k in (2, 1, 3):
-        O.arrive(O.near(k))
-        O.along_y(k).start()
-
-        @pl.when(middle)
+        attend_tile(4 * (i // 2) + 1 + i % 2)
+
+    @pl.when(middle)
+    def _():
+        for copy in state_sends[1:]:
+            copy.wait_send()
+
+        @pl.when(has_far)
         def _():
+            halo_far.wait_send()
+
+        for to in (w.to_z, w.to_zc):
+            pl.semaphore_signal(go, inc=1, device_id=to, device_id_type=MESH)
+
+    @pl.when(w.g == 0)
+    def _():
+        pl.semaphore_wait(go, 2)
+        for k in range(4):
+            if k:
+                pass_near(O, k)
             O.along_h(k).start()
 
-    @pl.loop(4, 8)
+    halo_arrive(pick(0, 0), pick(after_at, before_at), 0, w.to_y)
+    halo_arrive(pick(1, 0), pick(before_at, after_at), 1, w.to_y)
+    halo_arrive(pick(1, 1), pick(after_at, before_at), 2, w.to_y)
+
+    @pl.when(has_far)
+    def _():
+        halo_arrive(pick(0, 1), pick(before_at, after_at), 3, w.to_hy)
+
+    @pl.loop(0, 4)
     def _(i):
-        attend_tile(i)
+        attend_tile(4 * (i // 2) + 3 * (i % 2))
+
+    for i, here in enumerate((stall.at[1 - y], crossing.at[0], crossing.at[1])):
+        remote(here, here, st_sem.at[0, i], st_sem.at[1, i], w.to_y).wait_recv()
+    crossed = crossing[0].astype(f32) + crossing[1].astype(f32)
+    for slot in range(2):
+        for i in range(2):
+            total = jnp.where(w.zh == 1 - i, 1.0, 0.0) * coef[slot, 2, 0:1, :] * crossed
+            for s in range(2):
+                for yy in range(2):
+                    for zh in range(2):
+                        r = 4 * zh + 2 * s + yy
+                        total = total + coef[slot, i, r : r + 1, :] * stall[yy, s, i].astype(f32)
+            states[slot, :, i * H : (i + 1) * H] = total.astype(bf16)
+
+    def finish_tile(i):
+        slot = i // 2
+        at = pl.ds(pl.multiple_of(i * own, own), own)
+        column = cumc[slot, pl.ds(pl.multiple_of((i % 2) * own, own), own), :]
+        last = cumr[slot, 0:1, run_rows - 1 : run_rows]
+        carried = jnp.dot(rets[0, at, :], states[slot], preferred_element_type=f32)
+        value = (
+            acc_r[at, :H] + jnp.exp(column) * carried[:, :H]
+            + jnp.exp(last - column) * carried[:, H:]
+        )
+        value = value - jnp.mean(value, axis=1, keepdims=True)
+        value = value * lax.rsqrt(jnp.mean(value * value, axis=1, keepdims=True) + 1e-06)
+        value = value.astype(bf16)
+        out = pl.ds(pl.multiple_of(i * edge, edge), edge)
+        mix[0, out, 2 * H :] = value[:edge]
+        mix[1, out, 2 * H :] = value[edge:]
+
+    @pl.loop(0, 4)
+    def _(i):
+        finish_tile(i)
 
     turned = jnp.transpose(logm[...])
     for b in range(4):
@@ -574,126 +791,37 @@
         for i, (x, zl, to) in enumerate(log_to)
     ]
 
-    R.arrive_across()
-
-    def retention_inputs(b):
-        at = pl.ds(pl.multiple_of(b * own, own), own)
-        scale_b = inverse(b)
-        both = project(R, b, 0, 2 * H)
-        rets[0, at, :] = (both[:, :H] * scale_b).astype(bf16)
-        rets[1, at, :] = (both[:, H:] * (scale_b * H ** (-0.5))).astype(bf16)
-        rets[2, at, :] = (project(R, b, 2 * H, H) * scale_b).astype(bf16)
-
-    @pl.loop(0, 4)
-    def _(b):
-        retention_inputs(b)
-
-    for slot in range(2):
-        at = pl.ds(slot * run_rows, run_rows)
-        last = cumr[slot, 0:1, run_rows - 1 : run_rows]
-        key, value = rets[1, at, :].astype(f32), rets[2, at, :]
-        for i, weight in enumerate((jnp.exp(last - cumc[slot]), jnp.exp(cumc[slot]))):
-            lhs = (key * weight).astype(bf16)
-            state = lax.dot_general(
-                lhs, value, (((0,), (0,)), ((), ())), preferred_element_type=f32
-            ).astype(bf16)
-            stall[w.zh, w.y, slot, i] = state
-    state_sends = [
-        remote(
-            stall.at[w.zh, w.y], stall.at[w.zh, w.y], st_sem.at[0, i], st_sem.at[1, i], to
-        )
-        for i, to in enumerate((w.to_y, w.to_h, w.to_hy))
-    ]
-    for copy in state_sends:
-        copy.start()
     for copy in log_sends:
         copy.start()
 
-    @pl.when(w.g == 0)
-    def _():
-        for k in range(1, 4):
-            O.along_h(k).start()
-
-    def inner_tile(i):
-        slot = i // 2
-        at = pl.ds(pl.multiple_of(i * own, own), own)
-        keys = pl.ds(pl.multiple_of(slot * run_rows, run_rows), run_rows)
-        score = lax.dot_general(
-            rets[0, at, :], rets[1, keys, :], (((1,), (1,)), ((), ())),
-            preferred_element_type=f32,
-        )
-        column = cumc[slot, pl.ds(pl.multiple_of((i % 2) * own, own), own), :]
-        column = jnp.concatenate([column] * (run_rows // H), axis=1)
-        weight = jnp.exp(-jnp.abs(column - cumr[slot, 0:1, :]))
-        proj[at, :] = jnp.dot(
-            (score * weight).astype(bf16), rets[2, keys, :], preferred_element_type=f32
-        )
-
-    @pl.loop(0, 4)
-    def _(i):
-        inner_tile(i)
-
-    for i, (zh, yy) in enumerate(((w.zh, 1 - y), (1 - w.zh, y), (1 - w.zh, 1 - y))):
-        here = stall.at[zh, yy]
-        remote(here, here, st_sem.at[0, i], st_sem.at[1, i], w.to_y).wait_recv()
-    for slot in range(2):
-        for i in range(2):
-            total = jnp.zeros((H, H), f32)
-            for zh in range(2):
-                for s in range(2):
-                    for yy in range(2):
-                        r = 4 * zh + 2 * s + yy
-                        total = total + coef[slot, i, r : r + 1, :] * stall[
-                            zh, yy, s, i
-                        ].astype(f32)
-            states[slot, :, i * H : (i + 1) * H] = total.astype(bf16)
-
-    def finish_tile(i):
-        slot = i // 2
-        at = pl.ds(pl.multiple_of(i * own, own), own)
-        column = cumc[slot, pl.ds(pl.multiple_of((i % 2) * own, own), own), :]
-        last = cumr[slot, 0:1, run_rows - 1 : run_rows]
-        carried = jnp.dot(rets[0, at, :], states[slot], preferred_element_type=f32)
-        value = (
-            proj[at, :] + jnp.exp(column) * carried[:, :H]
-            + jnp.exp(last - column) * carried[:, H:]
-        )
-        value = value - jnp.mean(value, axis=1, keepdims=True)
-        value = value * lax.rsqrt(jnp.mean(value * value, axis=1, keepdims=True) + 1e-06)
-        value = value.astype(bf16)
-        out = pl.ds(pl.multiple_of(i * edge, edge), edge)
-        mix[0, out, 2 * H :] = value[:edge]
-        mix[1, out, 2 * H :] = value[edge:]
-
-    @pl.loop(0, 4)
-    def _(i):
-        finish_tile(i)
-
-    for k in range(4):
-        pass_far(O, k)
-
     chunks = 8
 
     def columns_of(i, x):
-        a, far, zl = i // 4, (i // 2) % 2, i % 2
-        yy = a + y - 2 * a * y
-        zh = far + w.zh - 2 * far * w.zh
-        return w.at(zh, zl, yy, x)
+        far, across, zl = i // 4, (i // 2) % 2, i % 2
+        return w.at(flip(w.zh, far), zl, flip(y, across), x)
 
     def swap(i):
         return remote(give.at[i], take.at[i], give_s.at[i], take_r.at[i], w.to_c)
 
-    def first_hop(i):
-        return (
-            remote(s1.at[i, 0], r1.at[i, 0], s1_s.at[i, 0], r1_r.at[i, 0], w.to_x),
-            remote(s1.at[i, 1], r1.at[i, 1], s1_s.at[i, 1], r1_r.at[i, 1], w.to_z),
-        )
-
-    def second_hop(i):
-        return (
-            remote(s2.at[i, 0], r2.at[i, 0], s2_s.at[i, 0], r2_r.at[i, 0], w.to_z),
-            remote(s2.at[i, 1], r2.at[i, 1], s2_s.at[i, 1], r2_r.at[i, 1], w.to_x),
-        )
+    def x_first(i, k):
+        return 1 if k == 0 else jnp.where(i < 2, 1, 0)
+
+    def toward(dx):
+        return {"x": flip(w.x, dx), "zl": flip(w.zl, 1 - dx)}
+
+    def first_hop(i, k):
+        to = toward(x_first(i, k))
+        return remote(s1.at[i, k], r1.at[i, k], s1_s.at[i, k], r1_r.at[i, k], to)
+
+    def second_hop(i, k):
+        to = toward(1 - x_first(i, k))
+        return remote(s2.at[i, k], r2.at[i, k], s2_s.at[i, k], r2_r.at[i, k], to)
+
+    def side(i, k, j, cross):
+        dx = x_first(i, k)
+        zl = dx * j + (1 - dx) * flip(w.zl, cross)
+        x = dx * flip(w.x, cross) + (1 - dx) * j
+        return block(zl, x)
 
     def part(b):
         return pl.ds(pl.multiple_of(b * edge, edge), edge)
@@ -704,10 +832,20 @@
         def _():
             i = step
 
-            @pl.when(i >= chunks // 2)
+            @pl.when((i // 2) % 2 == 1)
             def _():
                 for x in range(2):
                     O.arrive(columns_of(i, x))
+
+            @pl.when((i == 1) & (w.g == 0))
+            def _():
+                for k in range(2):
+                    pass_far(O, k)
+
+            @pl.when(i == 3)
+            def _():
+                for k in range(2, 4):
+                    pass_far(O, k)
 
             for k in range(2):
                 give[i, k] = jnp.dot(
@@ -715,7 +853,7 @@
                 ).astype(bf16)
             swap(i).start()
             for k in range(2):
-                mine[i, k] = jnp.dot(
+                mine[i % 4, k] = jnp.dot(
                     mix[w.c], O.wide[columns_of(i, k)], preferred_element_type=f32
                 )
 
@@ -725,37 +863,36 @@
             swap(i).wait_recv()
             for k in range(2):
                 for j in range(2):
-                    b = block(j, 1 - w.x) if k == 0 else block(1 - w.zl, j)
-                    total = mine[i, k, part(b), :] + take[i, k, part(b), :].astype(f32)
+                    b = side(i, k, j, 1)
+                    total = mine[i % 4, k, part(b), :] + take[i, k, part(b), :].astype(f32)
                     s1[i, k, j] = total.astype(bf16)
-            for copy in first_hop(i):
-                copy.start()
+                first_hop(i, k).start()
             for k in range(2):
                 for j in range(2):
-                    b = block(j, w.x) if k == 0 else block(w.zl, j)
-                    mine[i, k, part(b), :] += take[i, k, part(b), :].astype(f32)
+                    b = side(i, k, j, 0)
+                    mine[i % 4, k, part(b), :] += take[i, k, part(b), :].astype(f32)
 
         @pl.when((step >= 2) & (step < chunks + 2))
         def _():
             i = step - 2
-            for k, copy in enumerate(first_hop(i)):
-                copy.wait_recv()
-                b = block(1 - w.zl, w.x) if k == 0 else block(w.zl, 1 - w.x)
-                j = 1 - w.zl if k == 0 else 1 - w.x
-                s2[i, k] = (mine[i, k, part(b), :] + r1[i, k, j].astype(f32)).astype(bf16)
-                second_hop(i)[k].start()
             for k in range(2):
-                j = w.zl if k == 0 else w.x
-                mine[i, k, part(w.b), :] += r1[i, k, j].astype(f32)
+                first_hop(i, k).wait_recv()
+                dx = x_first(i, k)
+                j = flip(dx * w.zl + (1 - dx) * w.x, 1)
+                b = side(i, k, j, 0)
+                s2[i, k] = (mine[i % 4, k, part(b), :] + r1[i, k, j].astype(f32)).astype(bf16)
+                second_hop(i, k).start()
 
         @pl.when(step >= 3)
         def _():
             i = step - 3
-            for k, copy in enumerate(second_hop(i)):
-                copy.wait_recv()
+            for k in range(2):
+                second_hop(i, k).wait_recv()
+                dx = x_first(i, k)
+                j = dx * w.zl + (1 - dx) * w.x
                 at = pl.ds(pl.multiple_of(columns_of(i, k) * own, own), own)
-                total = mine[i, k, part(w.b), :] + r2[i, k].astype(f32)
-                mixed[:, at] = total.astype(mixed.dtype)
+                total = mine[i % 4, k, part(w.b), :] + r1[i, k, j].astype(f32)
+                mixed[:, at] = (total + r2[i, k].astype(f32)).astype(mixed.dtype)
 
     for i, (x, zl, to) in enumerate(log_to):
         here = lrecv.at[h_of(zl, x)]
@@ -769,24 +906,28 @@
 
     for stream in (A, R, O):
         stream.drain()
-    for k in range(4):
-        tokens_c(k).wait_send()
     for i in range(1, 16):
         decay_send(i).wait_send()
-    for copy in tokens_x + (tokens_z, gain_c):
+    for copy in tokens_x + tokens_c + [tokens_z, gain_c]:
         copy.wait_send()
-    for copy in halo_y + state_sends + log_sends:
+    for copy in halo_y + state_sends[:1] + log_sends:
         copy.wait_send()
 
-    @pl.when(has_far)
-    def _():
-        halo_far.wait_send()
+    @pl.when(w.g == 0)
+    def _():
+        for copy in state_sends[1:]:
+            copy.wait_send()
+
+        @pl.when(has_far)
+        def _():
+            halo_far.wait_send()
 
     @pl.loop(0, chunks)
     def _(i):
         swap(i).wait_send()
-        for copy in first_hop(i) + second_hop(i):
-            copy.wait_send()
+        for k in range(2):
+            first_hop(i, k).wait_send()
+            second_hop(i, k).wait_send()
 
 
 def fused(*args):
@@ -832,25 +973,26 @@
             vmem((2, rows, half_d), bf16),
             vmem((2, rows, H), f32),
             vmem((2, 1, half_d), f32),
-            vmem((rows, H), f32),
+            vmem((rows, 4 * H), f32),
+            vmem((rows, 3 * H), f32),
             vmem((2, 2, run_rows + 2 * edge, H), bf16),
             vmem((rows, 2 * H), bf16),
             vmem((3, rows, H), bf16),
             vmem((2, 2, 2, 2) + decay_log.shape, f32),
             vmem((2, 8, run_rows), f32),
             vmem((2, run_rows, H), f32),
-            vmem((2, 2, 8, H), f32),
+            vmem((2, 3, 8, H), f32),
             vmem((2, H, 2 * H), bf16),
-            vmem((2, 2, 2, 2, H, H), bf16),
+            vmem((2, 2, 2, H, H), bf16), vmem((3, H, H), bf16),
             vmem((2, 4 * edge, 3 * H), bf16),
             vmem((2 * edge, H), f32),
             vmem((4, 2, 2 * edge), f32),
             vmem((4, 2, 2 * edge), f32),
-            vmem(tile, f32), vmem(tile, bf16), vmem(tile, bf16),
+            vmem((4,) + tile[1:], f32), vmem(tile, bf16), vmem(tile, bf16),
             vmem((8, 2, 2, edge, own), bf16), vmem((8, 2, 2, edge, own), bf16),
             vmem((8, 2, edge, own), bf16), vmem((8, 2, edge, own), bf16),
-            dma((3,)), dma((2,)), dma((1,)), dma((4,)), dma((2, 4)), dma((2,)), dma((2, 16)),
-            dma((2, 4)), dma((2, 3)), dma((2, 3)),
+            dma((3,)), dma((3,)), dma((1,)), dma((5,)), dma((2, 4, 2)), dma((2,)), dma((2, 16)),
+            dma((2, 4)), dma((2, 3)), dma((2, 3)), pltpu.SemaphoreType.REGULAR,
             dma((8,)), dma((8,)), dma((8, 2)), dma((8, 2)), dma((8, 2)), dma((8, 2)),
         ]
         + stream((depth, 4 * H))

time: 189 us -> 170 us (0.90)
  Pallas kernels: 185 us -> 166 us
    pallas_call x1, Pallas kernels: 185 us -> 166 us  [fused(): pl.pallas_call(fused_kernel, out_shape=(jax.ShapeDtypeStruct((own // 2, w...]
where the time goes in v3:
time: 170 us
  Pallas kernels  166 us (98%)
  local copies, waits for them, and re-layouts  2.9 us (2%)
    pallas_call x1, Pallas kernels, fused(): pl.pallas_call(fused_kernel, out_shape=(jax.ShapeDtypeStruct((own // 2, w...  166 us

profile of v3, /device:TPU:0, one launch (start us, length us, event | category | flops | bytes accessed | tf_op | source)
XLA Modules:
  0.0 169.6 jit_solution(2529577145456163568)
XLA Ops:
  0.6 166.1 %shard_map.158 = (bf16[128,4096]{1,0:T(8,128)(2,1)}, f32[8,256]{1,0:T(8,128)}) custom-call(bf16[256,2048]{1,0:T(8,128)(2,1)} %tokens.1, f32[1,2048]{1,0:T(1,128)} %bitcast.1, bf16[256,1024]{1,0:T(8,128)(2,1)} %q_att.1, bf16[256,512]{1,0:T(8,128)(2,1)} %k_att.1, bf16[256,512]{1,0:T(8,128)(2,1)} %v_att.1, bf16[256,512]{1,0:T(8,128)(2,1)} %q_ret.1, ...), custom_call_target="tpu_custom_call" | custom-call | flops 99999997952 | bytes 20000000 | tf_op jit(solution)/shard_map/pallas_call | solution.py:963
  166.7 0.0 copy-start
  166.7 2.3 %copy.19 = bf16[128,4096]{1,0:T(8,128)(2,1)} copy(bf16[128,4096]{1,0:T(8,128)(2,1)} %get-tuple-element.4) | data formatting | bytes 2097152
  169.0 0.0 copy-done
  169.0 0.6 copy.20
Async XLA Ops:
  166.7 2.3 %copy-start = (f32[8,256]{1,0:T(8,128)S(1)}, f32[8,256]{1,0:T(8,128)}, u32[]{:S(2)}) copy-start(f32[8,256]{1,0:T(8,128)} %get-tuple-element.5) | copy-start | bytes 24580

commit v4 on v3

--- a/solution.py
+++ b/solution.py
@@ -49,13 +49,26 @@
     return v + bit - 2 * v * bit
 
 
+class Both:
+    def __init__(self, *copies):
+        self.copies = copies
+
+    def start(self):
+        for copy in self.copies:
+            copy.start()
+
+    def wait_send(self):
+        for copy in self.copies:
+            copy.wait_send()
+
+
 class Stream:
-    def __init__(self, where, remote, refs, pack):
-        self.where, self.remote, self.pack = where, remote, pack
+    def __init__(self, where, remote, refs, pack, split=False):
+        self.where, self.remote, self.pack, self.split = where, remote, pack, split
         (
             self.wide, self.away, self.out,
             self.load, self.x_send, self.z_send, self.h_send, self.y_send,
-            self.p_recv, self.w_recv,
+            self.p_recv, self.w_recv, self.more_recv,
         ) = refs
 
     def fetch(self):
@@ -106,18 +119,57 @@
         w = self.where
         return w.at(1 - w.zh, flip(w.zl, 1 - k // 2), 1 - w.y, flip(w.x, k % 2))
 
+    def half(self, s, i):
+        rows = self.wide.shape[1] // 2
+        return self.wide.at[s, pl.ds(i * rows, rows), :]
+
+    def halves(self, s, sends, hop, to):
+        recvs = (self.w_recv.at[s], self.more_recv.at[hop])
+        return [
+            self.remote(self.half(s, i), self.half(s, i), sends[i], recvs[i], to)
+            for i in range(2)
+        ]
+
     def along_h(self, k):
         s = self.near(k)
+        if self.split and k == 3:
+            return Both(
+                *self.halves(s, (self.h_send.at[3], self.h_send.at[4]), 0, self.where.to_h)
+            )
         return self.remote(
             self.wide.at[s], self.wide.at[s], self.h_send.at[k], self.w_recv.at[s], self.where.to_h
         )
 
     def along_y(self, k, far=0):
         s = self.far(k) if far else self.near(k)
+        if self.split and far and k == 3:
+            return Both(
+                *self.halves(s, (self.y_send.at[7], self.y_send.at[8]), 1, self.where.to_y)
+            )
         return self.remote(
             self.wide.at[s], self.wide.at[s],
             self.y_send.at[4 * far + k], self.w_recv.at[s], self.where.to_y,
         )
+
+    def pass_far(self, k):
+        if self.split and k == 3:
+            sends = (self.h_send.at[3], self.h_send.at[4])
+            arrivals = self.halves(self.far(k), sends, 0, self.where.to_h)
+            for arrival, copy in zip(arrivals, self.along_y(k, 1).copies):
+                arrival.wait_recv()
+                copy.start()
+        else:
+            self.arrive(self.far(k))
+            self.along_y(k, 1).start()
+
+    def arrive_far_across(self, k):
+        s = self.across(k)
+        if self.split and k == 3:
+            sends = (self.y_send.at[7], self.y_send.at[8])
+            for arrival in self.halves(s, sends, 1, self.where.to_y):
+                arrival.wait_recv()
+        else:
+            self.arrive(s)
 
     def arrive(self, s):
         self.remote(
@@ -174,7 +226,7 @@
     cos_t, sin_t, base,
     mixed, logs_out,
     raw, scl, ssq, gains, acc_a, acc_r, kvext, qrot, rets, dec, cumr, cumc, coef, states, stall, crossing,
-    mix, logm, lsend, lrecv, mine, give, take, s1, r1, s2, r2,
+    mix, bias, logm, lsend, lrecv, mine, kept, give, take, s1, r1, s2, r2,
     t_load, t_x, t_z, t_c, t_recv, g_sem, d_sem, halo_sem, st_sem, l_sem, go,
     give_s, take_r, s1_s, r1_r, s2_s, r2_r,
     *streams,
@@ -221,7 +273,7 @@
         return pack
 
     n = len(streams) // 3
-    A = Stream(w, remote, streams[:n], pack_cols((q_att, k_att, v_att)))
+    A = Stream(w, remote, streams[:n], pack_cols((q_att, k_att, v_att)), True)
     R = Stream(w, remote, streams[n : 2 * n], pack_cols((q_ret, k_ret, v_ret)))
     O = Stream(w, remote, streams[2 * n :], pack_rows((out_att, out_ret)))
 
@@ -349,8 +401,7 @@
             stream.along_h(k).start()
 
     def pass_far(stream, k):
-        stream.arrive(stream.far(k))
-        stream.along_y(k, 1).start()
+        stream.pass_far(k)
 
     pass_near(R, 2)
     pass_near(A, 2)
@@ -371,6 +422,10 @@
     def _():
         O.along_h(0).start()
 
+    row = lax.broadcasted_iota(jnp.int32, bias.shape, 0)
+    shift = lax.broadcasted_iota(jnp.int32, bias.shape, 1) - lax.rem(row, edge)
+    bias[...] = jnp.where((shift >= 0) & (shift <= 2 * edge), 0.0, -jnp.inf)
+    logm[...] = jnp.zeros_like(logm)
     for i in range(1, 16):
         decay_arrive(i)
 
@@ -407,9 +462,10 @@
         factor = jnp.exp(jnp.sum(jnp.where(between, totals, 0.0), axis=1, keepdims=True))
         coef[slot, 2] = jnp.broadcast_to(factor, (8, H))
 
+    pass_near(O, 1)
+
     @pl.when(middle)
     def _():
-        pass_near(O, 1)
         for stream in (R, A):
             for k in (0, 2, 1, 3):
                 pass_far(stream, k)
@@ -559,7 +615,7 @@
     def _():
         pass_far(A, 2)
 
-    @pl.loop(0, 4)
+    @pl.loop(0, 4, unroll=True)
     def _(b):
         retention_inputs(b)
 
@@ -600,7 +656,7 @@
             (score * weight).astype(bf16), rets[2, keys, :], preferred_element_type=f32
         )
 
-    @pl.loop(0, 4)
+    @pl.loop(0, 4, unroll=True)
     def _(i):
         inner_tile(i)
 
@@ -613,17 +669,16 @@
         add_pair(A, acc_a, i // 4, y, i % 4)
 
     for k in range(2):
-        A.arrive(A.across(k))
+        A.arrive_far_across(k)
 
     @pl.loop(0, 4)
     def _(b):
         add_pair(A, acc_a, 1 - w.zl, 1 - y, b)
 
-    state_sends[0].start()
     for k in range(2, 4):
-        A.arrive(A.across(k))
-
-    @pl.loop(0, 4)
+        A.arrive_far_across(k)
+
+    @pl.loop(0, 4, unroll=True)
     def _(b):
         keys_values(b)
 
@@ -660,14 +715,28 @@
     def _():
         halo_far.start()
 
+    state_sends[0].start()
+
     @pl.when(middle)
     def _():
+        for copy in state_sends[1:]:
+            copy.wait_send()
+
+        @pl.when(has_far)
+        def _():
+            halo_far.wait_send()
+
+        for to in (w.to_z, w.to_zc):
+            pl.semaphore_signal(go, inc=1, device_id=to, device_id_type=MESH)
+
+    @pl.when(middle)
+    def _():
         for k in (2, 3):
-            pass_near(O, k)
-        for k in range(2):
-            pass_far(O, k)
-
-    @pl.loop(0, 4)
+            O.arrive(O.near(k))
+            O.along_h(k).start()
+            O.along_y(k).start()
+
+    @pl.loop(0, 4, unroll=True)
     def _(b):
         queries(b)
 
@@ -675,7 +744,7 @@
         here = piece(slot, start)
         remote(here, here, halo_sem.at[0, i], halo_sem.at[1, i], to).wait_recv()
 
-    def attend_tile(i):
+    def attend_tile(i, at_end):
         slot, j = i // 4, i % 4
         query = qrot[pl.ds(pl.multiple_of(i * edge, edge), edge), :]
         query = jnp.concatenate([query[:, :H], query[:, H:]], axis=0)
@@ -684,14 +753,12 @@
         score = lax.dot_general(
             query, key, (((1,), (1,)), ((), ())), preferred_element_type=f32
         ) * H ** (-0.5)
-        row = lax.broadcasted_iota(jnp.int32, score.shape, 0)
-        col = lax.broadcasted_iota(jnp.int32, score.shape, 1)
-        shift = col - jnp.where(row < edge, row, row - edge)
-        start = w.at(w.zh, slot, y, 0) * own + j * edge - edge
-        valid = (
-            (shift >= 0) & (shift <= 2 * edge) & (col >= -start) & (col < total_rows - start)
-        )
-        masked = jnp.where(valid, score, -jnp.inf)
+        masked = score + bias[...]
+        if at_end:
+            col = lax.broadcasted_iota(jnp.int32, (1, 3 * edge), 1)
+            start = w.at(w.zh, slot, y, 0) * own + j * edge - edge
+            inside = (col >= -start) & (col < total_rows - start)
+            masked = masked + jnp.where(inside, 0.0, -jnp.inf)
         first = lax.broadcasted_iota(jnp.int32, (2 * edge, 1), 0) < edge
         limit = jnp.where(first, sink[2 * w.h], sink[2 * w.h + 1])
         top = jnp.maximum(jnp.max(masked, axis=1, keepdims=True), limit)
@@ -706,31 +773,17 @@
         column = lax.broadcasted_iota(jnp.int32, (2 * edge, H), 1)
         logm[...] = jnp.where(column == i, logs, logm[...])
 
-    logm[...] = jnp.zeros_like(logm)
-
-    @pl.loop(0, 4)
-    def _(i):
-        attend_tile(4 * (i // 2) + 1 + i % 2)
-
-    @pl.when(middle)
-    def _():
-        for copy in state_sends[1:]:
-            copy.wait_send()
-
-        @pl.when(has_far)
-        def _():
-            halo_far.wait_send()
-
-        for to in (w.to_z, w.to_zc):
-            pl.semaphore_signal(go, inc=1, device_id=to, device_id_type=MESH)
-
     @pl.when(w.g == 0)
     def _():
         pl.semaphore_wait(go, 2)
         for k in range(4):
-            if k:
-                pass_near(O, k)
+            if k > 1:
+                O.arrive(O.near(k))
             O.along_h(k).start()
+
+    @pl.loop(0, 4, unroll=True)
+    def _(i):
+        attend_tile(4 * (i // 2) + 1 + i % 2, False)
 
     halo_arrive(pick(0, 0), pick(after_at, before_at), 0, w.to_y)
     halo_arrive(pick(1, 0), pick(before_at, after_at), 1, w.to_y)
@@ -740,9 +793,14 @@
     def _():
         halo_arrive(pick(0, 1), pick(before_at, after_at), 3, w.to_hy)
 
-    @pl.loop(0, 4)
+    @pl.when(w.g == 0)
+    def _():
+        O.along_y(2).start()
+        O.along_y(3).start()
+
+    @pl.loop(0, 4, unroll=True)
     def _(i):
-        attend_tile(4 * (i // 2) + 3 * (i % 2))
+        attend_tile(4 * (i // 2) + 3 * (i % 2), True)
 
     for i, here in enumerate((stall.at[1 - y], crossing.at[0], crossing.at[1])):
         remote(here, here, st_sem.at[0, i], st_sem.at[1, i], w.to_y).wait_recv()
@@ -774,9 +832,14 @@
         mix[0, out, 2 * H :] = value[:edge]
         mix[1, out, 2 * H :] = value[edge:]
 
-    @pl.loop(0, 4)
+    @pl.loop(0, 4, unroll=True)
     def _(i):
         finish_tile(i)
+
+    @pl.when(middle)
+    def _():
+        for k in range(2):
+            pass_far(O, k)
 
     turned = jnp.transpose(logm[...])
     for b in range(4):
@@ -804,7 +867,7 @@
         return remote(give.at[i], take.at[i], give_s.at[i], take_r.at[i], w.to_c)
 
     def x_first(i, k):
-        return 1 if k == 0 else jnp.where(i < 2, 1, 0)
+        return 1 if k == 0 else jnp.where(i < 1, 1, 0)
 
     def toward(dx):
         return {"x": flip(w.x, dx), "zl": flip(w.zl, 1 - dx)}
@@ -826,7 +889,9 @@
     def part(b):
         return pl.ds(pl.multiple_of(b * edge, edge), edge)
 
-    @pl.loop(0, chunks + 3)
+    lag = 6
+
+    @pl.loop(0, chunks + lag)
     def _(step):
         @pl.when(step < chunks)
         def _():
@@ -837,7 +902,7 @@
                 for x in range(2):
                     O.arrive(columns_of(i, x))
 
-            @pl.when((i == 1) & (w.g == 0))
+            @pl.when((i == 2) & (w.g == 0))
             def _():
                 for k in range(2):
                     pass_far(O, k)
@@ -882,17 +947,16 @@
                 b = side(i, k, j, 0)
                 s2[i, k] = (mine[i % 4, k, part(b), :] + r1[i, k, j].astype(f32)).astype(bf16)
                 second_hop(i, k).start()
-
-        @pl.when(step >= 3)
+                j = flip(j, 1)
+                kept[i, k] = mine[i % 4, k, part(w.b), :] + r1[i, k, j].astype(f32)
+
+        @pl.when(step >= lag)
         def _():
-            i = step - 3
+            i = step - lag
             for k in range(2):
                 second_hop(i, k).wait_recv()
-                dx = x_first(i, k)
-                j = dx * w.zl + (1 - dx) * w.x
                 at = pl.ds(pl.multiple_of(columns_of(i, k) * own, own), own)
-                total = mine[i % 4, k, part(w.b), :] + r1[i, k, j].astype(f32)
-                mixed[:, at] = (total + r2[i, k].astype(f32)).astype(mixed.dtype)
+                mixed[:, at] = (kept[i, k] + r2[i, k].astype(f32)).astype(mixed.dtype)
 
     for i, (x, zl, to) in enumerate(log_to):
         here = lrecv.at[h_of(zl, x)]
@@ -954,13 +1018,13 @@
     def stream(block):
         return [
             vmem((16,) + block, bf16), vmem((2,) + block, bf16), vmem((2,) + block, bf16),
-            dma((4,)), dma((2,)), dma((2,)), dma((4,)), dma((8,)), dma((1,)), dma((16,)),
+            dma((4,)), dma((2,)), dma((2,)), dma((5,)), dma((9,)), dma((1,)), dma((16,)), dma((2,)),
         ]
 
     out_rows = (out_att.shape[0] + out_ret.shape[0]) // 4
     tile = (8, 2, 4 * edge, own)
     hbm, inside = pl.BlockSpec(memory_space=pl.ANY), pl.BlockSpec(memory_space=pltpu.VMEM)
-    return pl.pallas_call(
+    mixed, logs = pl.pallas_call(
         fused_kernel,
         out_shape=(
             jax.ShapeDtypeStruct((own // 2, width), bf16),
@@ -985,10 +1049,11 @@
             vmem((2, H, 2 * H), bf16),
             vmem((2, 2, 2, H, H), bf16), vmem((3, H, H), bf16),
             vmem((2, 4 * edge, 3 * H), bf16),
+            vmem((2 * edge, 3 * edge), f32),
             vmem((2 * edge, H), f32),
             vmem((4, 2, 2 * edge), f32),
             vmem((4, 2, 2 * edge), f32),
-            vmem((4,) + tile[1:], f32), vmem(tile, bf16), vmem(tile, bf16),
+            vmem((4,) + tile[1:], f32), vmem((8, 2, edge, own), f32), vmem(tile, bf16), vmem(tile, bf16),
             vmem((8, 2, 2, edge, own), bf16), vmem((8, 2, 2, edge, own), bf16),
             vmem((8, 2, edge, own), bf16), vmem((8, 2, edge, own), bf16),
             dma((3,)), dma((3,)), dma((1,)), dma((5,)), dma((2, 4, 2)), dma((2,)), dma((2, 16)),
@@ -1007,6 +1072,7 @@
     )(
         tokens, gain.reshape(1, half_d), *args[2:10], sink, decay_log, cos_t, sin_t, base
     )
+    return mixed, logs
 
 
 def attend(query, key, value, sink, offset, total_rows):

time: 170 us -> 166 us (0.976)
  Pallas kernels: 166 us -> 162 us
    pallas_call x1, Pallas kernels: 166 us -> 162 us  [fused(): pl.pallas_call(fused_kernel, out_shape=(jax.ShapeDtypeStruct((own // 2, w...]
where the time goes in v4:
time: 166 us
  Pallas kernels  162 us (98%)
  local copies, waits for them, and re-layouts  2.9 us (2%)
    pallas_call x1, Pallas kernels, fused(): pl.pallas_call(fused_kernel, out_shape=(jax.ShapeDtypeStruct((own // 2, w...  162 us

profile of v4, /device:TPU:0, one launch (start us, length us, event | category | flops | bytes accessed | tf_op | source)
XLA Modules:
  0.0 165.7 jit_solution(10150991322279693777)
XLA Ops:
  0.6 162.1 %shard_map.158 = (bf16[128,4096]{1,0:T(8,128)(2,1)}, f32[8,256]{1,0:T(8,128)}) custom-call(bf16[256,2048]{1,0:T(8,128)(2,1)} %tokens.1, f32[1,2048]{1,0:T(1,128)} %bitcast.1, bf16[256,1024]{1,0:T(8,128)(2,1)} %q_att.1, bf16[256,512]{1,0:T(8,128)(2,1)} %k_att.1, bf16[256,512]{1,0:T(8,128)(2,1)} %v_att.1, bf16[256,512]{1,0:T(8,128)(2,1)} %q_ret.1, ...), custom_call_target="tpu_custom_call" | custom-call | flops 99999997952 | bytes 20000000 | tf_op jit(solution)/shard_map/pallas_call | solution.py:1027
  162.7 0.0 copy-start
  162.8 2.3 %copy.19 = bf16[128,4096]{1,0:T(8,128)(2,1)} copy(bf16[128,4096]{1,0:T(8,128)(2,1)} %get-tuple-element.4) | data formatting | bytes 2097152
  165.0 0.0 copy-done
  165.1 0.6 copy.20
Async XLA Ops:
  162.7 2.3 %copy-start = (f32[8,256]{1,0:T(8,128)S(1)}, f32[8,256]{1,0:T(8,128)}, u32[]{:S(2)}) copy-start(f32[8,256]{1,0:T(8,128)} %get-tuple-element.5) | copy-start | bytes 24580

commit v5 on v4

--- a/solution.py
+++ b/solution.py
@@ -49,6 +49,9 @@
     return v + bit - 2 * v * bit
 
 
+PARTS = 2
+
+
 class Both:
     def __init__(self, *copies):
         self.copies = copies
@@ -68,7 +71,7 @@
         (
             self.wide, self.away, self.out,
             self.load, self.x_send, self.z_send, self.h_send, self.y_send,
-            self.p_recv, self.w_recv, self.more_recv,
+            self.p_recv, self.w_recv, self.more_send, self.more_recv,
         ) = refs
 
     def fetch(self):
@@ -119,42 +122,36 @@
         w = self.where
         return w.at(1 - w.zh, flip(w.zl, 1 - k // 2), 1 - w.y, flip(w.x, k % 2))
 
-    def half(self, s, i):
-        rows = self.wide.shape[1] // 2
-        return self.wide.at[s, pl.ds(i * rows, rows), :]
-
-    def halves(self, s, sends, hop, to):
-        recvs = (self.w_recv.at[s], self.more_recv.at[hop])
+    def parts_of(self, s, hop, k, to):
+        rows = self.wide.shape[1] // PARTS
+        pieces = [self.wide.at[s, pl.ds(i * rows, rows), :] for i in range(PARTS)]
         return [
-            self.remote(self.half(s, i), self.half(s, i), sends[i], recvs[i], to)
-            for i in range(2)
+            self.remote(
+                piece, piece, self.more_send.at[hop, k, i], self.more_recv.at[hop, k, i], to
+            )
+            for i, piece in enumerate(pieces)
         ]
 
     def along_h(self, k):
         s = self.near(k)
-        if self.split and k == 3:
-            return Both(
-                *self.halves(s, (self.h_send.at[3], self.h_send.at[4]), 0, self.where.to_h)
-            )
+        if self.split:
+            return Both(*self.parts_of(s, 0, k, self.where.to_h))
         return self.remote(
             self.wide.at[s], self.wide.at[s], self.h_send.at[k], self.w_recv.at[s], self.where.to_h
         )
 
     def along_y(self, k, far=0):
         s = self.far(k) if far else self.near(k)
-        if self.split and far and k == 3:
-            return Both(
-                *self.halves(s, (self.y_send.at[7], self.y_send.at[8]), 1, self.where.to_y)
-            )
+        if far and self.split:
+            return Both(*self.parts_of(s, 1, k, self.where.to_y))
         return self.remote(
             self.wide.at[s], self.wide.at[s],
             self.y_send.at[4 * far + k], self.w_recv.at[s], self.where.to_y,
         )
 
     def pass_far(self, k):
-        if self.split and k == 3:
-            sends = (self.h_send.at[3], self.h_send.at[4])
-            arrivals = self.halves(self.far(k), sends, 0, self.where.to_h)
+        if self.split:
+            arrivals = self.parts_of(self.far(k), 0, k, self.where.to_h)
             for arrival, copy in zip(arrivals, self.along_y(k, 1).copies):
                 arrival.wait_recv()
                 copy.start()
@@ -164,9 +161,8 @@
 
     def arrive_far_across(self, k):
         s = self.across(k)
-        if self.split and k == 3:
-            sends = (self.y_send.at[7], self.y_send.at[8])
-            for arrival in self.halves(s, sends, 1, self.where.to_y):
+        if self.split:
+            for arrival in self.parts_of(s, 1, k, self.where.to_y):
                 arrival.wait_recv()
         else:
             self.arrive(s)
@@ -274,7 +270,7 @@
 
     n = len(streams) // 3
     A = Stream(w, remote, streams[:n], pack_cols((q_att, k_att, v_att)), True)
-    R = Stream(w, remote, streams[n : 2 * n], pack_cols((q_ret, k_ret, v_ret)))
+    R = Stream(w, remote, streams[n : 2 * n], pack_cols((q_ret, k_ret, v_ret)), True)
     O = Stream(w, remote, streams[2 * n :], pack_rows((out_att, out_ret)))
 
     token_load = pltpu.make_async_copy(tokens, raw.at[w.c, w.b], t_load.at[0])
@@ -535,17 +531,19 @@
 
     R.arrive_across(0)
     A.arrive_across(0)
-
-    @pl.loop(0, 3)
-    def _(i):
-        k = 2 - i
-        b = block(flip(w.zl, k // 2), flip(w.x, k % 2))
-        first_part(R, acc_r, b)
-        first_part(A, acc_a, b)
+    for k in (2, 0):
+        first_part(R, acc_r, order(k))
+        first_part(A, acc_a, order(k))
 
     @pl.when(w.g == 0)
     def _():
         pass_far(R, 2)
+
+    first_part(R, acc_r, order(1))
+    first_part(A, acc_a, order(1))
+    @pl.when(w.g == 0)
+    def _():
+        pass_far(R, 3)
 
     token_arrive(3, None, 0)
     tokens_c[3].start()
@@ -555,7 +553,6 @@
 
     @pl.when(w.g == 0)
     def _():
-        pass_far(R, 3)
         pass_far(A, 0)
 
     token_arrive(3, None, 1)
@@ -601,7 +598,8 @@
         qrot[at, :H] = turn(query[:, :H], cosine, sine)
         qrot[at, H:] = turn(query[:, H:], cosine, sine)
 
-    R.arrive_across(1)
+    for k in range(4):
+        R.arrive_far_across(k)
 
     def retention_inputs(b):
         at = pl.ds(pl.multiple_of(b * own, own), own)
@@ -907,7 +905,7 @@
                 for k in range(2):
                     pass_far(O, k)
 
-            @pl.when(i == 3)
+            @pl.when(i == 4)
             def _():
                 for k in range(2, 4):
                     pass_far(O, k)
@@ -994,6 +992,31 @@
             second_hop(i, k).wait_send()
 
 
+def settle_kernel(mixed, logs, mixed_out, logs_out, sems):
+    rows = mixed.shape[0] // 8
+    copies = [
+        pltpu.make_async_copy(
+            mixed.at[pl.ds(i * rows, rows)], mixed_out.at[pl.ds(i * rows, rows)], sems.at[i]
+        )
+        for i in range(8)
+    ]
+    copies.append(pltpu.make_async_copy(logs, logs_out, sems.at[8]))
+    for copy in copies:
+        copy.start()
+    for copy in copies:
+        copy.wait()
+
+
+def settle(mixed, logs):
+    return pl.pallas_call(
+        settle_kernel,
+        out_shape=tuple(jax.ShapeDtypeStruct(v.shape, v.dtype) for v in (mixed, logs)),
+        in_specs=[pl.BlockSpec(memory_space=pltpu.VMEM)] * 2,
+        out_specs=[pl.BlockSpec(memory_space=pl.ANY)] * 2,
+        scratch_shapes=[pltpu.SemaphoreType.DMA((9,))],
+    )(mixed, logs)
+
+
 def fused(*args):
     tokens, gain, q_att = args[:3]
     out_att, out_ret, sink, decay_log = args[8:]
@@ -1018,7 +1041,8 @@
     def stream(block):
         return [
             vmem((16,) + block, bf16), vmem((2,) + block, bf16), vmem((2,) + block, bf16),
-            dma((4,)), dma((2,)), dma((2,)), dma((5,)), dma((9,)), dma((1,)), dma((16,)), dma((2,)),
+            dma((4,)), dma((2,)), dma((2,)), dma((4,)), dma((8,)), dma((1,)), dma((16,)),
+            dma((2, 4, PARTS)), dma((2, 4, PARTS)),
         ]
 
     out_rows = (out_att.shape[0] + out_ret.shape[0]) // 4
@@ -1072,7 +1096,7 @@
     )(
         tokens, gain.reshape(1, half_d), *args[2:10], sink, decay_log, cos_t, sin_t, base
     )
-    return mixed, logs
+    return settle(mixed, logs)
 
 
 def attend(query, key, value, sink, offset, total_rows):

time: 166 us -> 165 us (level)
  local copies, waits for them, and re-layouts: 2.9 us -> 0 us
  Pallas kernels: 162 us -> 164 us
    unnamed x4 -> x0, local copies, waits for them, and re-layouts: 2.9 us -> none
    pallas_call x0 -> x1, Pallas kernels: none -> 2.26 us  [settle(): pl.pallas_call(settle_kernel, out_shape=tuple((jax.ShapeDtypeStruct(v.sha...]
where the time goes in v5:
time: 165 us
  Pallas kernels  164 us (99%)
    pallas_call x1, Pallas kernels, fused(): pl.pallas_call(fused_kernel, out_shape=(jax.ShapeDtypeStruct((own // 2, w...  161 us

profile of v5, /device:TPU:0, one launch (start us, length us, event | category | flops | bytes accessed | tf_op | source)
XLA Modules:
  0.0 164.5 jit_solution(15129055098225685504)
XLA Ops:
  0.6 161.5 %shard_map.158 = (bf16[128,4096]{1,0:T(8,128)(2,1)}, f32[8,256]{1,0:T(8,128)}) custom-call(bf16[256,2048]{1,0:T(8,128)(2,1)} %tokens.1, f32[1,2048]{1,0:T(1,128)} %bitcast.1, bf16[256,1024]{1,0:T(8,128)(2,1)} %q_att.1, bf16[256,512]{1,0:T(8,128)(2,1)} %k_att.1, bf16[256,512]{1,0:T(8,128)(2,1)} %v_att.1, bf16[256,512]{1,0:T(8,128)(2,1)} %q_ret.1, ...), custom_call_target="tpu_custom_call" | custom-call | flops 99999997952 | bytes 20000000 | tf_op jit(solution)/shard_map/pallas_call | solution.py:1051
  162.1 2.3 %shard_map.159 = (bf16[128,4096]{1,0:T(8,128)(2,1)}, f32[8,256]{1,0:T(8,128)}) custom-call(bf16[128,4096]{1,0:T(8,128)(2,1)} %get-tuple-element.4.mixed, f32[8,256]{1,0:T(8,128)} %get-tuple-element.5.logs), custom_call_target="tpu_custom_call" | custom-call | tf_op jit(solution)/shard_map/pallas_call | solution.py:1011

commit v6 on v5

--- a/solution.py
+++ b/solution.py
@@ -891,35 +891,6 @@
 
     @pl.loop(0, chunks + lag)
     def _(step):
-        @pl.when(step < chunks)
-        def _():
-            i = step
-
-            @pl.when((i // 2) % 2 == 1)
-            def _():
-                for x in range(2):
-                    O.arrive(columns_of(i, x))
-
-            @pl.when((i == 2) & (w.g == 0))
-            def _():
-                for k in range(2):
-                    pass_far(O, k)
-
-            @pl.when(i == 4)
-            def _():
-                for k in range(2, 4):
-                    pass_far(O, k)
-
-            for k in range(2):
-                give[i, k] = jnp.dot(
-                    mix[1 - w.c], O.wide[columns_of(i, k)], preferred_element_type=f32
-                ).astype(bf16)
-            swap(i).start()
-            for k in range(2):
-                mine[i % 4, k] = jnp.dot(
-                    mix[w.c], O.wide[columns_of(i, k)], preferred_element_type=f32
-                )
-
         @pl.when((step >= 1) & (step < chunks + 1))
         def _():
             i = step - 1
@@ -934,6 +905,35 @@
                 for j in range(2):
                     b = side(i, k, j, 0)
                     mine[i % 4, k, part(b), :] += take[i, k, part(b), :].astype(f32)
+
+        @pl.when(step < chunks)
+        def _():
+            i = step
+
+            @pl.when((i // 2) % 2 == 1)
+            def _():
+                for x in range(2):
+                    O.arrive(columns_of(i, x))
+
+            @pl.when((i == 2) & (w.g == 0))
+            def _():
+                for k in range(2):
+                    pass_far(O, k)
+
+            @pl.when(i == 4)
+            def _():
+                for k in range(2, 4):
+                    pass_far(O, k)
+
+            for k in range(2):
+                give[i, k] = jnp.dot(
+                    mix[1 - w.c], O.wide[columns_of(i, k)], preferred_element_type=f32
+                ).astype(bf16)
+            swap(i).start()
+            for k in range(2):
+                mine[i % 4, k] = jnp.dot(
+                    mix[w.c], O.wide[columns_of(i, k)], preferred_element_type=f32
+                )
 
         @pl.when((step >= 2) & (step < chunks + 2))
         def _():

time: 165 us -> 165 us (level)
  no operation moved by 1% of the time
where the time goes in v6:
time: 165 us
  Pallas kernels  164 us (99%)
    pallas_call x1, Pallas kernels, fused(): pl.pallas_call(fused_kernel, out_shape=(jax.ShapeDtypeStruct((own // 2, w...  161 us

profile of v6, /device:TPU:0, one launch (start us, length us, event | category | flops | bytes accessed | tf_op | source)
XLA Modules:
  0.0 164.5 jit_solution(8444154227556749502)
XLA Ops:
  0.6 161.5 %shard_map.158 = (bf16[128,4096]{1,0:T(8,128)(2,1)}, f32[8,256]{1,0:T(8,128)}) custom-call(bf16[256,2048]{1,0:T(8,128)(2,1)} %tokens.1, f32[1,2048]{1,0:T(1,128)} %bitcast.1, bf16[256,1024]{1,0:T(8,128)(2,1)} %q_att.1, bf16[256,512]{1,0:T(8,128)(2,1)} %k_att.1, bf16[256,512]{1,0:T(8,128)(2,1)} %v_att.1, bf16[256,512]{1,0:T(8,128)(2,1)} %q_ret.1, ...), custom_call_target="tpu_custom_call" | custom-call | flops 99999997952 | bytes 20000000 | tf_op jit(solution)/shard_map/pallas_call | solution.py:1051
  162.1 2.3 %shard_map.159 = (bf16[128,4096]{1,0:T(8,128)(2,1)}, f32[8,256]{1,0:T(8,128)}) custom-call(bf16[128,4096]{1,0:T(8,128)(2,1)} %get-tuple-element.4.mixed, f32[8,256]{1,0:T(8,128)} %get-tuple-element.5.logs), custom_call_target="tpu_custom_call" | custom-call | tf_op jit(solution)/shard_map/pallas_call | solution.py:1011
